TPU v7x, 512 devices: a 8x2x16 block of a 8x8x16 slice. The times are simulated.
512 devices in a mesh: grp: 2 (over y), ep: 32 (over z, core), tp: 8 (over x).
Axes of the slice: x: 8, y: 2, z: 16, core: 2. Of those that a mesh axis runs over, the one named last changes fastest.
The devices are a block of a 8x8x16 slice.
Arguments:
- tokens: bfloat16 [640, 1024], P(('grp', 'ep')), parts along dimension 0, may hold values from -40 to 40
- attn_gain: float32 [1024], replicated, may hold values from 0.1 to 1.9
- w_query: bfloat16 [1024, 1024], P(None, 'tp'), may hold values from -0.1875 to 0.1875
- w_key: bfloat16 [1024, 512], P(None, 'tp'), may hold values from -0.1875 to 0.1875
- w_value: bfloat16 [1024, 512], P(None, 'tp'), may hold values from -0.1875 to 0.1875
- key_cache: bfloat16 [640, 512, 1024], P(('grp', 'ep'), 'tp'), parts along dimension 0, may hold values from -6 to 6
- value_cache: bfloat16 [640, 512, 1024], P(('grp', 'ep'), 'tp'), parts along dimension 0, may hold values from -6 to 6
- lengths: int32 [640], P(('grp', 'ep')), parts along dimension 0, may hold values from 256 to 1024
- head_bias: float32 [16], P('tp'), may hold values from -8 to -2
- w_out: bfloat16 [1024, 1024], P(None, 'tp'), may hold values from -0.1875 to 0.1875
- ffn_gain: float32 [1024], replicated, may hold values from 0.1 to 1.9
- route_ids: int32 [640, 2], P(('grp', 'ep')), parts along dimension 0, may hold values from 0 to 31, all different within a row; in each aligned block of 10 rows (0 to 9, 10 to 19, ...) at most 2 rows name the same one
- route_weights: float32 [640, 2], P(('grp', 'ep')), parts along dimension 0, may hold values from 0.1 to 1
- w_gate: bfloat16 [32, 1024, 2048], P('ep', None, 'tp'), may hold values from -0.1875 to 0.1875
- w_up: bfloat16 [32, 1024, 2048], P('ep', None, 'tp'), may hold values from -0.1875 to 0.1875
- w_down: bfloat16 [32, 2048, 1024], P('ep', 'tp'), may hold values from -0.125 to 0.125
Outputs:
- mixed: bfloat16 [640, 1024], P(('grp', 'ep'), 'tp'), parts along dimension 0
- new_keys: bfloat16 [640, 512], P(('grp', 'ep'), 'tp'), parts along dimension 0
- new_values: bfloat16 [640, 512], P(('grp', 'ep'), 'tp'), parts along dimension 0
There are 2 independent parts, one for each index of `grp`. A program takes and returns all parts, laid end to end along the dimension named above; an argument that names none is the same for every part. Nothing has to cross between parts.
Inputs may be any that keep to these rules, and one draw needn't show every extreme that they name: `route_ids`: each row names 2 different experts. In each aligned block of 10 rows no expert is named more than 2 times, and in some block some expert is named exactly 2 times.
All inputs are finite; a program needn't handle non-finite values.
Results may differ from a plain program's by a relative error of at most 0.012.
Values may be sent and summed in bfloat16 or wider, within the bound.
A program may use at most 64 MiB of HBM per device.

v0:
```python
import jax
import jax.numpy as jnp
from jax import lax
from jax.sharding import PartitionSpec as P

HEAD_SIZE = 64


epsilon = 1e-06


def in_blocks(array, dim, devices):
    shape = array.shape
    blocks = array.reshape(*shape[:dim], devices, shape[dim] // devices, *shape[dim + 1 :])
    return jnp.moveaxis(blocks, dim, 0)


def sum_at_owner(array, axis, dim):
    blocks = in_blocks(array, dim, lax.axis_size(axis))
    arrived = lax.all_to_all(blocks, axis, split_axis=0, concat_axis=0, tiled=True)
    return arrived.astype(jnp.float32).sum(axis=0)


def copy_for_each(array, axis):
    copies = jnp.broadcast_to(array, (lax.axis_size(axis), *array.shape))
    return lax.all_to_all(copies, axis, split_axis=0, concat_axis=0, tiled=True)


def laid_out(blocks, dim):
    blocks = jnp.moveaxis(blocks, 0, dim)
    shape = blocks.shape
    return blocks.reshape(*shape[:dim], shape[dim] * shape[dim + 1], *shape[dim + 2 :])


def gathered_copies(array, axis, dim):
    blocks = copy_for_each(array, axis)
    return laid_out(blocks, dim)


def expert_block(arrived, w_gate, w_up, w_down):
    gate_act = jnp.einsum("erd,edf->erf", arrived, w_gate, preferred_element_type=jnp.float32)
    up_act = jnp.einsum("erd,edf->erf", arrived, w_up, preferred_element_type=jnp.float32)
    hidden_act = (jax.nn.silu(gate_act) * up_act).astype(jnp.bfloat16)
    partial_value = jnp.einsum(
        "erf,efd->erd", hidden_act, w_down, preferred_element_type=jnp.float32
    )
    return sum_at_owner(partial_value.astype(jnp.bfloat16), "tp", 2).astype(jnp.bfloat16)


def slot_places(pair_expert, first_expert, experts_here, capacity):
    pair_count = pair_expert.shape[0]
    local_expert = pair_expert - first_expert
    expert_hits = (
        local_expert[:, None] == lax.broadcasted_iota(jnp.int32, (1, experts_here), 1)
    ).astype(jnp.int32)
    before = jnp.cumsum(expert_hits, axis=0) - expert_hits
    slot_rank = jnp.sum(before * expert_hits, axis=1)
    is_here = jnp.sum(expert_hits, axis=1) > 0
    slot_index = jnp.where(is_here, local_expert * capacity + slot_rank, -1)
    slot_count = experts_here * capacity
    return (
        lax.broadcasted_iota(jnp.int32, (slot_count, pair_count), 0) == slot_index[None, :]
    ).astype(jnp.bfloat16)


def later_sum(log_rest):
    lead = log_rest.shape[:-1]
    cache_len = log_rest.shape[-1]
    block_len = 128
    block_count = cache_len // block_len
    blocks = log_rest.reshape(lead + (block_count, block_len))
    inner_tri = (
        lax.broadcasted_iota(jnp.int32, (block_len, block_len), 0)
        > lax.broadcasted_iota(jnp.int32, (block_len, block_len), 1)
    ).astype(jnp.float32)
    within = jnp.einsum("...bj,jp->...bp", blocks, inner_tri)
    totals = jnp.sum(blocks, axis=-1)
    outer_tri = (
        lax.broadcasted_iota(jnp.int32, (block_count, block_count), 0)
        > lax.broadcasted_iota(jnp.int32, (block_count, block_count), 1)
    ).astype(jnp.float32)
    carried = jnp.einsum("...c,cb->...b", totals, outer_tri)
    return (within + carried[..., None]).reshape(lead + (cache_len,))


def shards(
    tokens,
    attn_gain,
    w_query,
    w_key,
    w_value,
    key_cache,
    value_cache,
    lengths,
    head_bias,
    w_out,
    ffn_gain,
    route_ids,
    route_weights,
    w_gate,
    w_up,
    w_down,
):
    seq_rows, model_width = tokens.shape
    query_cols = w_query.shape[1]
    key_cols = w_key.shape[1]
    token_rows = tokens.astype(jnp.float32)
    normed = (
        token_rows
        * lax.rsqrt(jnp.mean(token_rows * token_rows, axis=1, keepdims=True) + epsilon)
        * attn_gain
    ).astype(jnp.bfloat16)
    queries = jnp.dot(normed, w_query, preferred_element_type=jnp.float32).astype(jnp.bfloat16)
    new_keys = jnp.dot(normed, w_key, preferred_element_type=jnp.float32).astype(jnp.bfloat16)
    new_values = jnp.dot(normed, w_value, preferred_element_type=jnp.float32).astype(jnp.bfloat16)
    kv_local = key_cols // HEAD_SIZE
    group_size = query_cols // key_cols
    cache_len = key_cache.shape[2]
    query_heads = queries.reshape(seq_rows, kv_local, group_size, HEAD_SIZE)
    key_heads = key_cache.reshape(seq_rows, kv_local, HEAD_SIZE, cache_len)
    value_heads = value_cache.reshape(seq_rows, kv_local, HEAD_SIZE, cache_len)
    scores = jnp.einsum(
        "skgd,skdl->skgl", query_heads, key_heads, preferred_element_type=jnp.float32
    ) * HEAD_SIZE ** (-0.5)
    scores = scores + head_bias.reshape(kv_local, group_size)[None, :, :, None]
    in_cache = (
        lax.broadcasted_iota(jnp.int32, (seq_rows, 1, 1, cache_len), 3)
        < lengths[:, None, None, None]
    )
    log_rest = jnp.where(in_cache, jax.nn.log_sigmoid(-scores), 0.0)
    tail_sum = later_sum(log_rest)
    breaks = jnp.where(in_cache, jnp.exp(jax.nn.log_sigmoid(scores) + tail_sum), 0.0).astype(
        jnp.bfloat16
    )
    heads_out = jnp.einsum(
        "skgl,skdl->skgd", breaks, value_heads, preferred_element_type=jnp.float32
    )
    heads_out = heads_out.astype(jnp.bfloat16).reshape(seq_rows, query_cols)
    slice_width = w_out.shape[1]
    attn_out = jnp.dot(
        gathered_copies(heads_out, "tp", 1), w_out, preferred_element_type=jnp.float32
    )
    first_feature = lax.axis_index("tp") * slice_width
    own_tokens = lax.dynamic_slice_in_dim(token_rows, first_feature, slice_width, 1)
    own_hidden = own_tokens + attn_out
    full_hidden = gathered_copies(own_hidden, "tp", 1)
    whole_normed = (
        full_hidden
        * lax.rsqrt(jnp.mean(full_hidden * full_hidden, axis=1, keepdims=True) + epsilon)
        * ffn_gain
    ).astype(jnp.bfloat16)
    top_count = route_ids.shape[1]
    ep_count = lax.axis_size("ep")
    experts_here = w_gate.shape[0]
    expert_count = experts_here * ep_count
    capacity = min(seq_rows, max(2, (2 * seq_rows * top_count + expert_count - 1) // expert_count))
    pair_count = seq_rows * top_count
    slot_count = expert_count * capacity
    placing = slot_places(route_ids.reshape(pair_count), 0, expert_count, capacity)
    pair_rows = jnp.repeat(whole_normed, top_count, axis=0)
    outgoing = jnp.dot(placing, pair_rows, preferred_element_type=jnp.float32).astype(jnp.bfloat16)
    outgoing = outgoing.reshape(ep_count, experts_here, capacity, model_width)
    arrived = lax.all_to_all(outgoing, "ep", split_axis=0, concat_axis=2, tiled=True).reshape(
        experts_here, ep_count * capacity, model_width
    )
    expert_out = expert_block(arrived, w_gate, w_up, w_down)
    expert_out = expert_out.reshape(experts_here, ep_count, capacity, slice_width)
    returned_rows = lax.all_to_all(
        expert_out, "ep", split_axis=1, concat_axis=0, tiled=True
    ).reshape(slot_count, slice_width)
    picked = jnp.dot(placing.T, returned_rows, preferred_element_type=jnp.float32)
    routed_sum = jnp.sum(
        picked.reshape(seq_rows, top_count, slice_width) * route_weights[:, :, None], axis=1
    )
    mixed = (own_hidden + routed_sum).astype(jnp.bfloat16)
    return (mixed, new_keys, new_values)


def solution(mesh):
    in_specs = (
        P(("grp", "ep"), None),
        P(),
        P(None, "tp"),
        P(None, "tp"),
        P(None, "tp"),
        P(("grp", "ep"), "tp", None),
        P(("grp", "ep"), "tp", None),
        P(("grp", "ep")),
        P("tp"),
        P(None, "tp"),
        P(),
        P(("grp", "ep"), None),
        P(("grp", "ep"), None),
        P("ep", None, "tp"),
        P("ep", None, "tp"),
        P("ep", "tp", None),
    )
    out_specs = (P(("grp", "ep"), "tp"), P(("grp", "ep"), "tp"), P(("grp", "ep"), "tp"))
    return jax.shard_map(shards, mesh=mesh, in_specs=in_specs, out_specs=out_specs, check_vma=False)
```

profile of v0, /device:TPU:80, one launch (start us, length us, event | category | flops | bytes accessed | tf_op | source)
XLA Modules:
  0.0 127.7 jit_solution(9903634835739669839)
XLA Ops:
  0.6 0.0 copy-start
  0.6 1.0 multiply_reduce_fusion.1
  1.6 1.2 convolution_convert_fusion.5
  2.8 0.1 reshape.217
  2.9 0.7 iota_compare_fusion.1
  3.7 0.0 copy-done
  3.7 0.0 copy-start.8
  3.7 1.2 fusion.13
  4.8 0.1 reshape.218
  4.9 0.1 reduce_sum.67
  5.0 0.1 fusion.23
  5.2 0.1 copy.25
  5.3 0.0 copy-start.5
  5.3 0.2 convolution_add_fusion
  5.4 0.0 copy-start.4
  5.5 0.0 copy-done.8
  5.5 0.0 copy-start.6
  5.5 0.5 convolution_convert_fusion.2
  6.0 0.1 reshape.220
  6.1 0.6 broadcast_in_dim.36
  6.7 7.3 %all-to-all-start = ((bf16[8,10,128]{2,1,0:T(8,128)(2,1)}), bf16[8,10,128]{2,1,0:T(8,128)(2,1)S(1)}, u32[]{:S(2)}, u32[]{:S(2)}) async-start(bf16[8,10,128]{2,1,0:T(8,128)(2,1)} %broadcast_in_dim.36), calls=%async_computation | async-start | bytes 65536 | tf_op jit(solution)/shard_map/all_to_all | solution.py:26
  14.0 0.0 copy-done.7
  14.0 0.1 copy.27
  14.1 0.1 eq.36
  14.2 0.1 fusion.27
  14.3 0.2 select_reduce_fusion
  14.5 0.0 copy-done.5
  14.6 7.5 %all-to-all-done = bf16[8,10,128]{2,1,0:T(8,128)(2,1)S(1)} async-done(((bf16[8,10,128]{2,1,0:T(8,128)(2,1)}), bf16[8,10,128]{2,1,0:T(8,128)(2,1)S(1)}, u32[]{:S(2)}, u32[]{:S(2)}) %all-to-all-start) | async-done | bytes 20512 | tf_op jit(solution)/shard_map/all_to_all | solution.py:26
  22.1 0.0 copy-done.4
  22.1 0.2 convolution_add_fusion.1
  22.3 0.6 broadcast_in_dim.38
  22.9 3.6 %all-to-all-start.1 = ((f32[8,10,128]{2,1,0:T(8,128)}), f32[8,10,128]{2,1,0:T(8,128)S(1)}, u32[]{:S(2)}, u32[]{:S(2)}) async-start(f32[8,10,128]{2,1,0:T(8,128)} %broadcast_in_dim.38), calls=%async_computation.1 | async-start | bytes 131072 | tf_op jit(solution)/shard_map/all_to_all | solution.py:26
  26.5 8.1 %all-to-all-done.1 = f32[8,10,128]{2,1,0:T(8,128)S(1)} async-done(((f32[8,10,128]{2,1,0:T(8,128)}), f32[8,10,128]{2,1,0:T(8,128)S(1)}, u32[]{:S(2)}, u32[]{:S(2)}) %all-to-all-start.1) | async-done | bytes 40992 | tf_op jit(solution)/shard_map/all_to_all | solution.py:26
  34.6 0.1 multiply_reduce_fusion
  34.8 0.0 copy-done.6
  34.8 0.1 multiply_convert_fusion
  34.9 0.2 convolution_convert_fusion.1
  35.1 0.1 reshape.224
  35.2 60.8 %all_to_all.33 = bf16[32,1,2,1024]{3,2,1,0:T(2,128)(2,1)S(1)} all-to-all(bf16[32,1,2,1024]{3,2,1,0:T(2,128)(2,1)S(1)} %bitcast.55), channel_id=1, replica_groups=mesh['grp'=2,'ep'=32,'tp'=8] {'ep'}, dimensions={0} | all-to-all | bytes 262144 | tf_op jit(solution)/shard_map/all_to_all | solution.py:163
  95.9 0.1 reshape.225
  96.0 0.0 copy-done.1
  96.0 0.0 copy-start.9
  96.0 0.0 copy-start.11
  96.0 0.2 fusion.7
  96.2 0.0 copy-done.2
  96.2 0.0 copy-done.3
  96.2 0.0 copy-start.10
  96.2 0.0 copy-start.12
  96.3 0.5 fusion
  96.8 0.7 copy.41
  97.5 3.6 %all-to-all-start.3 = ((bf16[8,1,64,128]{3,2,1,0:T(8,128)(2,1)}), bf16[8,1,64,128]{3,2,1,0:T(8,128)(2,1)S(1)}, u32[]{:S(2)}, u32[]{:S(2)}) async-start(bf16[8,1,64,128]{3,2,1,0:T(8,128)(2,1)} %bitcast.53), calls=%async_computation.3 | async-start | bytes 262144 | tf_op jit(solution)/shard_map/all_to_all | solution.py:20
  101.0 0.0 copy-done.9
  101.0 0.0 copy-done.11
  101.1 0.8 convolution_convert_fusion.3
  101.9 0.0 copy-done.10
  101.9 0.8 convolution_convert_fusion.4
  102.7 7.2 %all-to-all-done.3 = bf16[8,1,64,128]{3,2,1,0:T(8,128)(2,1)S(1)} async-done(((bf16[8,1,64,128]{3,2,1,0:T(8,128)(2,1)}), bf16[8,1,64,128]{3,2,1,0:T(8,128)(2,1)S(1)}, u32[]{:S(2)}, u32[]{:S(2)}) %all-to-all-start.3) | async-done | bytes 131104 | tf_op jit(solution)/shard_map/all_to_all | solution.py:20
  109.9 0.6 reduce_sum.71
  110.5 4.8 %all-to-all-start.4 = ((bf16[1,32,2,128]{3,2,0,1:T(2,128)(2,1)}), bf16[1,32,2,128]{3,2,0,1:T(2,128)(2,1)S(1)}, u32[]{:S(2)}, u32[]{:S(2)}) async-start(bf16[1,32,2,128]{3,2,0,1:T(2,128)(2,1)} %bitcast.10), calls=%async_computation.4 | async-start | bytes 32768 | tf_op jit(solution)/shard_map/all_to_all | solution.py:168
  115.3 0.1 iota_compare_fusion.5
  115.4 11.6 %all-to-all-done.4 = bf16[1,32,2,128]{3,2,0,1:T(2,128)(2,1)S(1)} async-done(((bf16[1,32,2,128]{3,2,0,1:T(2,128)(2,1)}), bf16[1,32,2,128]{3,2,0,1:T(2,128)(2,1)S(1)}, u32[]{:S(2)}, u32[]{:S(2)}) %all-to-all-start.4) | async-done | bytes 16416 | tf_op jit(solution)/shard_map/all_to_all | solution.py:168
  127.0 0.0 copy-done.12
  127.0 0.1 fusion.3
  127.1 0.7 add_convert_fusion
  (20 shorter events, 0.3 us)
Async XLA Ops:
  0.6 3.0 %copy-start = (bf16[10,64,1024]{2,1,0:T(8,128)(2,1)S(1)}, bf16[10,64,1024]{2,1,0:T(8,128)(2,1)}, u32[]{:S(2)}) copy-start(bf16[10,64,1024]{2,1,0:T(8,128)(2,1)} %param.21) | copy-start | bytes 3932164
  3.7 1.8 %copy-start.8 = (bf16[10,64,1024]{2,1,0:T(8,128)(2,1)S(1)}, bf16[10,64,1024]{2,1,0:T(8,128)(2,1)}, u32[]{:S(2)}) copy-start(bf16[10,64,1024]{2,1,0:T(8,128)(2,1)} %param.22) | copy-start | bytes 3932164
  5.3 8.8 %copy-start.7 = (s32[10,2]{0,1:T(2,128)S(1)}, s32[10,2]{0,1:T(2,128)}, u32[]{:S(2)}) copy-start(s32[10,2]{0,1:T(2,128)} %param.27) | copy-start | bytes 244
  5.3 9.3 %copy-start.5 = (bf16[10,1024]{1,0:T(8,128)(2,1)S(1)}, bf16[10,1024]{1,0:T(8,128)(2,1)}, u32[]{:S(2)}) copy-start(bf16[10,1024]{1,0:T(8,128)(2,1)} %param.16) | copy-start | bytes 61444
  5.4 16.7 %copy-start.4 = (bf16[1024,128]{1,0:T(8,128)(2,1)S(1)}, bf16[1024,128]{1,0:T(8,128)(2,1)}, u32[]{:S(2)}) copy-start(bf16[1024,128]{1,0:T(8,128)(2,1)} %param.25) | copy-start | bytes 786436
  5.5 29.3 %copy-start.6 = (f32[1024]{0:T(1024)S(1)}, f32[1024]{0:T(1024)}, u32[]{:S(2)}) copy-start(f32[1024]{0:T(1024)} %param.26) | copy-start | bytes 12292
  6.1 89.9 %copy-start.1 = (bf16[1,1024,256]{2,1,0:T(8,128)(2,1)S(1)}, bf16[1,1024,256]{2,1,0:T(8,128)(2,1)}, u32[]{:S(2)}) copy-start(bf16[1,1024,256]{2,1,0:T(8,128)(2,1)} %param.29) | copy-start | bytes 1572868
  6.7 15.3 %all-to-all-start = ((bf16[8,10,128]{2,1,0:T(8,128)(2,1)}), bf16[8,10,128]{2,1,0:T(8,128)(2,1)S(1)}, u32[]{:S(2)}, u32[]{:S(2)}) async-start(bf16[8,10,128]{2,1,0:T(8,128)(2,1)} %broadcast_in_dim.36), calls=%async_computation | async-start | bytes 65536 | tf_op jit(solution)/shard_map/all_to_all | solution.py:26
  22.3 74.0 %copy-start.2 = (bf16[1,256,1024]{2,1,0:T(8,128)(2,1)S(1)}, bf16[1,256,1024]{2,1,0:T(8,128)(2,1)}, u32[]{:S(2)}) copy-start(bf16[1,256,1024]{2,1,0:T(8,128)(2,1)} %param.31) | copy-start | bytes 1572868
  22.3 74.0 %copy-start.3 = (bf16[1,1024,256]{2,1,0:T(8,128)(2,1)S(1)}, bf16[1,1024,256]{2,1,0:T(8,128)(2,1)}, u32[]{:S(2)}) copy-start(bf16[1,1024,256]{2,1,0:T(8,128)(2,1)} %param.30) | copy-start | bytes 1572868
  22.9 11.7 %all-to-all-start.1 = ((f32[8,10,128]{2,1,0:T(8,128)}), f32[8,10,128]{2,1,0:T(8,128)S(1)}, u32[]{:S(2)}, u32[]{:S(2)}) async-start(f32[8,10,128]{2,1,0:T(8,128)} %broadcast_in_dim.38), calls=%async_computation.1 | async-start | bytes 131072 | tf_op jit(solution)/shard_map/all_to_all | solution.py:26
  96.0 5.1 %copy-start.9 = (bf16[1024,64]{0,1:T(8,128)(2,1)S(1)}, bf16[1024,64]{0,1:T(8,128)(2,1)}, u32[]{:S(2)}) copy-start(bf16[1024,64]{0,1:T(8,128)(2,1)} %param.20) | copy-start | bytes 393220
  96.0 5.1 %copy-start.11 = (f32[1024]{0:T(1024)S(1)}, f32[1024]{0:T(1024)}, u32[]{:S(2)}) copy-start(f32[1024]{0:T(1024)} %param.17) | copy-start | bytes 12292
  96.2 5.6 %copy-start.10 = (bf16[1024,64]{0,1:T(8,128)(2,1)S(1)}, bf16[1024,64]{0,1:T(8,128)(2,1)}, u32[]{:S(2)}) copy-start(bf16[1024,64]{0,1:T(8,128)(2,1)} %param.19) | copy-start | bytes 393220
  96.2 30.8 %copy-start.12 = (f32[10,2]{0,1:T(2,128)S(1)}, f32[10,2]{0,1:T(2,128)}, u32[]{:S(2)}) copy-start(f32[10,2]{0,1:T(2,128)} %param.28) | copy-start | bytes 244
  97.5 12.4 %all-to-all-start.3 = ((bf16[8,1,64,128]{3,2,1,0:T(8,128)(2,1)}), bf16[8,1,64,128]{3,2,1,0:T(8,128)(2,1)S(1)}, u32[]{:S(2)}, u32[]{:S(2)}) async-start(bf16[8,1,64,128]{3,2,1,0:T(8,128)(2,1)} %bitcast.53), calls=%async_computation.3 | async-start | bytes 262144 | tf_op jit(solution)/shard_map/all_to_all | solution.py:20
  110.5 16.5 %all-to-all-start.4 = ((bf16[1,32,2,128]{3,2,0,1:T(2,128)(2,1)}), bf16[1,32,2,128]{3,2,0,1:T(2,128)(2,1)S(1)}, u32[]{:S(2)}, u32[]{:S(2)}) async-start(bf16[1,32,2,128]{3,2,0,1:T(2,128)(2,1)} %bitcast.10), calls=%async_computation.4 | async-start | bytes 32768 | tf_op jit(solution)/shard_map/all_to_all | solution.py:168
where the time goes:
time: 129 us; the launch traced here: 128 us
  blocking collectives  60.8 us (47%)
  waiting for transfers between devices  34.5 us (27%)
  starting transfers between devices  19.2 us (15%)
  matrix products  5.8 us (4%)
  other arithmetic  3.71 us (3%)
  local copies, waits for them, and re-layouts  2.78 us (2%)
    all_to_all x1, blocking collectives, shards(): lax.all_to_all(outgoing, 'ep', split_axis=0, concat_axis=2, tiled=True)  60.8 us
    all_to_all x2, waiting for transfers between devices, copy_for_each(): return lax.all_to_all(copies, axis, split_axis=0, concat_axis=0, tiled=True)  15.6 us
    all_to_all x1, waiting for transfers between devices, shards(): lax.all_to_all(expert_out, 'ep', split_axis=1, concat_axis=0, tiled=True)  11.6 us
    all_to_all x2, starting transfers between devices, copy_for_each(): return lax.all_to_all(copies, axis, split_axis=0, concat_axis=0, tiled=True)  10.9 us
    all_to_all x1, waiting for transfers between devices, sum_at_owner(): lax.all_to_all(blocks, axis, split_axis=0, concat_axis=0, tiled=True)  7.22 us
    all_to_all x1, starting transfers between devices, shards(): lax.all_to_all(expert_out, 'ep', split_axis=1, concat_axis=0, tiled=True)  4.77 us
    all_to_all x1, starting transfers between devices, sum_at_owner(): lax.all_to_all(blocks, axis, split_axis=0, concat_axis=0, tiled=True)  3.57 us
  transfers between devices with their start and end apart: 4, of which 4 were waited for; matrix products, arithmetic and copies ran while one was open for 2% of the time, Pallas kernels for 0%

commit v1 on v0

v1 whole, which is shorter than its diff:
```python
import functools

import jax
import jax.numpy as jnp
from jax import lax
from jax.experimental import pallas as pl
from jax.experimental.pallas import tpu as pltpu
from jax.sharding import PartitionSpec as P

HEAD_SIZE = 64
LANES = 128
CORES = 2
epsilon = 1e-06
f32 = jnp.float32
bf16 = jnp.bfloat16


def iota(shape, dim):
    return lax.broadcasted_iota(jnp.int32, shape, dim)


def hops(step, count):
    return min(step % count, -step % count)


def far_first(count):
    return sorted(range(1, count), key=lambda step: -hops(step, count))


def near_first(count):
    return sorted(range(1, count), key=lambda step: hops(step, count))


def nt_dot(left, right):
    return lax.dot_general(left, right, (((1,), (1,)), ((), ())), preferred_element_type=f32)


def kernel(
    n_tp,
    n_ep,
    tok_hbm,
    again_hbm,
    wq_hbm,
    wk_hbm,
    wv_hbm,
    key_hbm,
    val_hbm,
    len_hbm,
    bias_hbm,
    wo_hbm,
    fgain_hbm,
    ids_hbm,
    rw_hbm,
    wg_hbm,
    wu_hbm,
    wd_hbm,
    mixed_ref,
    nk_ref,
    nv_ref,
    tok,
    again,
    wq,
    wk,
    wv,
    key,
    val,
    lens,
    bias,
    wo,
    fgain,
    ids,
    rw,
    wg,
    wu,
    wd,
    rows_pad,
    idp,
    rwp,
    tri,
    place,
    combine,
    hid,
    hg,
    zsend,
    xg,
    rsend,
    rrecv,
    ysend,
    ret,
    local_sem,
    h_ssem,
    h_rsem,
    z_ssem,
    z_rsem,
    g_ssem,
    g_rsem,
    r_ssem,
    r_rsem,
    y_ssem,
    y_rsem,
):
    tp = lax.axis_index("tp")
    ep = lax.axis_index("ep")
    core = lax.rem(ep, CORES)
    chip = ep // CORES
    chips = n_ep // CORES
    half = n_ep // 2
    seq_rows = tok.shape[0]
    slots = 2 * n_ep

    barrier = pltpu.get_barrier_semaphore()
    for step in far_first(n_tp):
        pl.semaphore_signal(barrier, inc=1, device_id={"tp": lax.rem(tp + step, n_tp)})

    @pl.loop(1, n_ep)
    def _(step):
        pl.semaphore_signal(barrier, inc=1, device_id={"ep": lax.rem(ep + step, n_ep)})

    pairs = (
        (tok_hbm, tok),
        (again_hbm, again),
        (wq_hbm, wq),
        (len_hbm, lens),
        (bias_hbm, bias),
        (key_hbm, key),
        (ids_hbm, ids),
        (rw_hbm, rw),
        (val_hbm, val),
        (wo_hbm, wo),
        (fgain_hbm, fgain),
        (wk_hbm, wk),
        (wv_hbm, wv),
        (wg_hbm, wg),
        (wu_hbm, wu),
        (wd_hbm, wd),
    )
    copies = [
        pltpu.make_async_copy(source, target, local_sem.at[number])
        for number, (source, target) in enumerate(pairs)
    ]
    for copy in copies:
        copy.start()
    (
        c_tok, c_again, c_wq, c_len, c_bias, c_key, c_ids, c_rw,
        c_val, c_wo, c_fgain, c_wk, c_wv, c_wg, c_wu, c_wd,
    ) = copies

    def landed(view, sem):
        pltpu.make_async_copy(view, view, sem).wait()

    tri_len = tri.shape[0]
    tri[...] = (iota((tri_len, tri_len), 0) > iota((tri_len, tri_len), 1)).astype(f32).astype(bf16)
    rows_pad[...] = jnp.zeros_like(rows_pad)
    hid[...] = jnp.zeros_like(hid)
    idp[...] = jnp.full(idp.shape, -1.0, f32)
    rwp[...] = jnp.zeros_like(rwp)

    c_tok.wait()
    c_again.wait()
    token_rows = tok[...].astype(f32)
    mean_sq = jnp.mean(token_rows * token_rows, axis=1, keepdims=True)
    normed = (token_rows * lax.rsqrt(mean_sq + epsilon) * again[...]).astype(bf16)
    c_wq.wait()
    queries = jnp.dot(normed, wq[...], preferred_element_type=f32).astype(bf16).astype(f32)
    rows_pad[pl.ds(0, seq_rows), :] = queries * HEAD_SIZE ** (-0.5)
    padded = rows_pad[...]
    pad_rows = padded.shape[0]
    low = iota(padded.shape, 1) < HEAD_SIZE
    turned = pltpu.roll(padded, HEAD_SIZE, axis=1)
    both = jnp.concatenate([jnp.where(low, padded, turned), jnp.where(low, turned, padded)], axis=0)
    cols = key.shape[0]
    wide = jnp.concatenate([both] * (cols // LANES), axis=1)
    own_block = (iota(wide.shape, 1) // HEAD_SIZE) == lax.rem(iota(wide.shape, 0), pad_rows)
    spread = jnp.where(own_block, wide, 0.0).astype(bf16)

    c_len.wait()
    c_bias.wait()
    idp[pl.ds(2, 1), pl.ds(0, seq_rows)] = lens[...].astype(f32)
    len_row = jnp.broadcast_to(idp[pl.ds(2, 1), :], (2 * pad_rows, LANES))
    own_lane = iota(len_row.shape, 1) == lax.rem(iota(len_row.shape, 0), pad_rows)
    len_col = jnp.sum(jnp.where(own_lane, len_row, 0.0), axis=1, keepdims=True)
    bias_col = jnp.where(
        iota((2 * pad_rows, 1), 0) < pad_rows, bias[pl.ds(0, 1), pl.ds(0, 1)], bias[pl.ds(0, 1), pl.ds(1, 1)]
    )

    c_key.wait()
    scores = jnp.dot(spread, key[...], preferred_element_type=f32) + bias_col
    in_cache = iota(scores.shape, 1).astype(f32) < len_col
    log_rest = -(jnp.maximum(scores, 0.0) + jnp.log1p(jnp.exp(-jnp.abs(scores))))
    log_rest = jnp.where(in_cache, log_rest, 0.0)
    cache_len = scores.shape[1]
    chunk_count = cache_len // tri_len
    high = log_rest.astype(bf16)
    rest = (log_rest - high.astype(f32)).astype(bf16)
    stacked = jnp.concatenate(
        [part[:, c * tri_len : (c + 1) * tri_len] for part in (high, rest) for c in range(chunk_count)], axis=0
    )
    within = jnp.dot(stacked, tri[...], preferred_element_type=f32)
    tails = []
    carry = jnp.zeros((2 * pad_rows, 1), f32)
    span = 2 * pad_rows
    for c in reversed(range(chunk_count)):
        inner = within[c * span : (c + 1) * span] + within[(chunk_count + c) * span : (chunk_count + c + 1) * span]
        tails.append(inner + carry)
        carry = carry + inner[:, 0:1] + log_rest[:, c * tri_len : c * tri_len + 1]
    tail = jnp.concatenate(tails[::-1], axis=1)
    breaks = jnp.where(in_cache, jnp.exp(scores + log_rest + tail), 0.0).astype(bf16)
    c_val.wait()
    mixed_values = nt_dot(breaks, val[...])
    mixed_values = jnp.where(own_block, mixed_values, 0.0)
    folded = mixed_values[:, 0:LANES]
    for c in range(1, cols // LANES):
        folded = folded + mixed_values[:, c * LANES : (c + 1) * LANES]
    folded = folded + pltpu.roll(folded, HEAD_SIZE, axis=1)
    heads = jnp.where(low, folded[:pad_rows], folded[pad_rows:]).astype(bf16)
    hg[tp] = heads

    pl.semaphore_wait(barrier, (n_tp - 1) + (n_ep - 1))
    sends = []
    for step in far_first(n_tp):
        copy = pltpu.make_async_remote_copy(
            hg.at[tp], hg.at[tp], h_ssem.at[step], h_rsem.at[tp], device_id={"tp": lax.rem(tp + step, n_tp)}
        )
        copy.start()
        sends.append(copy)

    c_wk.wait()
    c_wv.wait()
    nk_ref[...] = nt_dot(normed, wk[...]).astype(bf16)
    nv_ref[...] = nt_dot(normed, wv[...]).astype(bf16)
    c_ids.wait()
    c_rw.wait()
    top_count = ids.shape[0]
    idp[pl.ds(0, top_count), pl.ds(0, seq_rows)] = ids[...].astype(f32)
    rwp[pl.ds(0, top_count), pl.ds(0, seq_rows)] = rw[...]
    slot_expert = (iota((slots, LANES), 0) // 2).astype(f32)
    slot_rank = lax.rem(iota((slots, LANES), 0), 2).astype(f32)
    hits = [(slot_expert == idp[pl.ds(k, 1), :]).astype(f32) for k in range(top_count)]
    any_hit = sum(hits)
    upper = (iota((LANES, LANES), 0) < iota((LANES, LANES), 1)).astype(f32).astype(bf16)
    before = jnp.dot(any_hit.astype(bf16), upper, preferred_element_type=f32)
    taken = jnp.where(before == slot_rank, 1.0, 0.0)
    place[...] = (any_hit * taken).astype(bf16)
    weighted = sum(hits[k] * rwp[pl.ds(k, 1), :] for k in range(top_count)) * taken
    weighted_t = weighted.T[: combine.shape[0] // 2]
    weighted_high = weighted_t.astype(bf16)
    combine[pl.ds(0, pad_rows), :] = weighted_high
    combine[pl.ds(pad_rows, pad_rows), :] = (weighted_t - weighted_high.astype(f32)).astype(bf16)
    c_fgain.wait()
    own_cols = pl.ds(pl.multiple_of(tp * LANES, LANES), LANES)
    own_tokens = tok[:, own_cols].astype(f32)
    own_gain = fgain[:, own_cols]

    c_wo.wait()
    attn_out = jnp.dot(hg[tp], wo[own_cols, :], preferred_element_type=f32)
    for step in near_first(n_tp):
        peer = lax.rem(tp + step, n_tp)
        landed(hg.at[peer], h_rsem.at[peer])
        attn_out += jnp.dot(
            hg[peer], wo[pl.ds(pl.multiple_of(peer * LANES, LANES), LANES), :], preferred_element_type=f32
        )
    hid[pl.ds(0, seq_rows), :] = own_tokens + attn_out[:seq_rows]
    scaled = (hid[...] * own_gain).astype(bf16)
    outgoing = jnp.dot(place[...], scaled, preferred_element_type=f32).astype(bf16)
    zsend[...] = outgoing.reshape(zsend.shape)

    for step in far_first(chips):
        for to_core in range(CORES):
            to_ep = lax.rem(chip + step, chips) * CORES + to_core
            at = ((chips - step + chips // 4 - 1) % chips) * CORES + core
            copy = pltpu.make_async_remote_copy(
                zsend.at[to_ep],
                xg.at[tp, at],
                z_ssem.at[step * CORES + to_core],
                z_rsem.at[at],
                device_id={"ep": to_ep},
            )
            copy.start()
            sends.append(copy)
    home = (chips // 4 - 1) * CORES
    partner = chip * CORES + (1 - core)
    copy = pltpu.make_async_remote_copy(
        zsend.at[partner], xg.at[tp, home + core], z_ssem.at[0], z_rsem.at[home + core], device_id={"ep": partner}
    )
    copy.start()
    sends.append(copy)
    xg[tp, home + core] = zsend[ep]

    for part in range(2):
        for number in range(half):
            at = part * half + number
            if at // CORES == home // CORES:
                continue
            landed(xg.at[tp, at], z_rsem.at[at])
        if part == 0:
            landed(xg.at[tp, home + 1 - core], z_rsem.at[home + 1 - core])
        span_at = pl.ds(part * half, half)
        for step in far_first(n_tp):
            copy = pltpu.make_async_remote_copy(
                xg.at[tp, span_at],
                xg.at[tp, span_at],
                g_ssem.at[part, step],
                g_rsem.at[part, tp],
                device_id={"tp": lax.rem(tp + step, n_tp)},
            )
            copy.start()
            sends.append(copy)

    c_wg.wait()
    c_wu.wait()
    c_wd.wait()
    gate = jnp.zeros((slots, wg.shape[1]), f32)
    up = jnp.zeros((slots, wu.shape[1]), f32)
    sum_sq = jnp.zeros((slots, 1), f32)
    for step in [0] + near_first(n_tp):
        peer = lax.rem(tp + step, n_tp)
        if step:
            for part in range(2):
                landed(xg.at[peer, pl.ds(part * half, half)], g_rsem.at[part, peer])
        rows = xg[peer].reshape(slots, LANES)
        peer_cols = pl.ds(pl.multiple_of(peer * LANES, LANES), LANES)
        gate += jnp.dot(rows, wg[peer_cols, :], preferred_element_type=f32)
        up += jnp.dot(rows, wu[peer_cols, :], preferred_element_type=f32)
        plain = rows.astype(f32) / fgain[:, peer_cols]
        sum_sq += jnp.sum(plain * plain, axis=1, keepdims=True)
    scale = lax.rsqrt(sum_sq / (n_tp * LANES) + epsilon)
    gate = gate * scale
    up = up * scale
    hidden_act = (gate / (1.0 + jnp.exp(-gate)) * up).astype(bf16)
    for part in (1, 0):
        act = hidden_act[part * slots // 2 : (part + 1) * slots // 2]
        partial_value = jnp.dot(act, wd[...], preferred_element_type=f32).astype(bf16)
        for c in range(n_tp):
            rsend[part, c] = partial_value[:, c * LANES : (c + 1) * LANES]
        for step in far_first(n_tp):
            peer = lax.rem(tp + step, n_tp)
            copy = pltpu.make_async_remote_copy(
                rsend.at[part, peer],
                rrecv.at[part, tp],
                r_ssem.at[part, step],
                r_rsem.at[part, tp],
                device_id={"tp": peer},
            )
            copy.start()
            sends.append(copy)

    for part in (1, 0):
        total = rsend[part, tp].astype(f32)
        for step in near_first(n_tp):
            peer = lax.rem(tp + step, n_tp)
            landed(rrecv.at[part, peer], r_rsem.at[part, peer])
            total += rrecv[part, peer].astype(f32)
        span_at = pl.ds(part * half, half)
        ysend[span_at] = total.astype(bf16).reshape(half, 2, LANES)
        order = range(half * part, half * (part + 1))
        order = sorted(order, key=lambda at: -hops((at - home) // CORES, chips))
        for at in order:
            step = at // CORES - home // CORES
            if step == 0:
                continue
            to_ep = lax.rem(chip + step + chips, chips) * CORES + at % CORES
            copy = pltpu.make_async_remote_copy(
                ysend.at[at], ret.at[ep], y_ssem.at[at], y_rsem.at[ep], device_id={"ep": to_ep}
            )
            copy.start()
            sends.append(copy)
        if part == 0:
            copy = pltpu.make_async_remote_copy(
                ysend.at[home + 1 - core], ret.at[ep], y_ssem.at[home], y_rsem.at[ep], device_id={"ep": partner}
            )
            copy.start()
            sends.append(copy)
            ret[ep] = ysend[home + core]

    for step in near_first(chips):
        for from_core in range(CORES):
            from_ep = lax.rem(chip + step, chips) * CORES + from_core
            landed(ret.at[from_ep], y_rsem.at[from_ep])
    landed(ret.at[partner], y_rsem.at[partner])
    picked = jnp.dot(combine[...], ret[...].reshape(slots, LANES), preferred_element_type=f32)
    routed_sum = picked[:pad_rows] + picked[pad_rows:]
    mixed_ref[...] = (hid[pl.ds(0, seq_rows), :] + routed_sum[:seq_rows]).astype(bf16)
    for copy in sends:
        copy.wait_send()


def shards(
    n_tp,
    n_ep,
    tokens,
    attn_gain,
    w_query,
    w_key,
    w_value,
    key_cache,
    value_cache,
    lengths,
    head_bias,
    w_out,
    ffn_gain,
    route_ids,
    route_weights,
    w_gate,
    w_up,
    w_down,
):
    seq_rows, model_width = tokens.shape
    cache_len = key_cache.shape[2]
    kv_cols = key_cache.shape[1]
    pad_rows = 16
    slots = 2 * n_ep
    operands = (
        tokens,
        attn_gain.reshape(1, model_width),
        w_query,
        w_key.T,
        w_value.T,
        key_cache.reshape(seq_rows * kv_cols, cache_len),
        value_cache.reshape(seq_rows * kv_cols, cache_len),
        lengths.reshape(1, seq_rows),
        head_bias.reshape(1, head_bias.shape[0]),
        w_out,
        ffn_gain.reshape(1, model_width),
        route_ids.T,
        route_weights.T,
        w_gate[0],
        w_up[0],
        w_down[0],
    )
    dma = pltpu.SemaphoreType.DMA
    scratch = [pltpu.VMEM(op.shape, op.dtype) for op in operands] + [
        pltpu.VMEM((pad_rows, LANES), f32),
        pltpu.VMEM((8, LANES), f32),
        pltpu.VMEM((8, LANES), f32),
        pltpu.VMEM((256, 256), bf16),
        pltpu.VMEM((slots, LANES), bf16),
        pltpu.VMEM((2 * pad_rows, slots), bf16),
        pltpu.VMEM((LANES, LANES), f32),
        pltpu.VMEM((n_tp, pad_rows, LANES), bf16),
        pltpu.VMEM((n_ep, 2, LANES), bf16),
        pltpu.VMEM((n_tp, n_ep, 2, LANES), bf16),
        pltpu.VMEM((2, n_tp, slots // 2, LANES), bf16),
        pltpu.VMEM((2, n_tp, slots // 2, LANES), bf16),
        pltpu.VMEM((n_ep, 2, LANES), bf16),
        pltpu.VMEM((n_ep, 2, LANES), bf16),
        dma((len(operands),)),
        dma((n_tp,)),
        dma((n_tp,)),
        dma((n_ep,)),
        dma((n_ep,)),
        dma((2, n_tp)),
        dma((2, n_tp)),
        dma((2, n_tp)),
        dma((2, n_tp)),
        dma((n_ep,)),
        dma((n_ep,)),
    ]
    return pl.pallas_call(
        functools.partial(kernel, n_tp, n_ep),
        out_shape=(
            jax.ShapeDtypeStruct((seq_rows, w_out.shape[1]), bf16),
            jax.ShapeDtypeStruct((seq_rows, w_key.shape[1]), bf16),
            jax.ShapeDtypeStruct((seq_rows, w_value.shape[1]), bf16),
        ),
        in_specs=[pl.BlockSpec(memory_space=pltpu.HBM)] * len(operands),
        out_specs=[pl.BlockSpec(memory_space=pltpu.VMEM)] * 3,
        scratch_shapes=scratch,
        compiler_params=pltpu.CompilerParams(collective_id=0, has_side_effects=True),
    )(*operands)


def solution(mesh):
    in_specs = (
        P(("grp", "ep"), None),
        P(),
        P(None, "tp"),
        P(None, "tp"),
        P(None, "tp"),
        P(("grp", "ep"), "tp", None),
        P(("grp", "ep"), "tp", None),
        P(("grp", "ep")),
        P("tp"),
        P(None, "tp"),
        P(),
        P(("grp", "ep"), None),
        P(("grp", "ep"), None),
        P("ep", None, "tp"),
        P("ep", None, "tp"),
        P("ep", "tp", None),
    )
    out_specs = (P(("grp", "ep"), "tp"), P(("grp", "ep"), "tp"), P(("grp", "ep"), "tp"))
    body = functools.partial(shards, mesh.shape["tp"], mesh.shape["ep"])
    return jax.shard_map(body, mesh=mesh, in_specs=in_specs, out_specs=out_specs, check_vma=False)
```

time: 129 us -> 84.9 us (0.66)
  Pallas kernels: 0 us -> 79.5 us
  blocking collectives: 60.8 us -> 0 us
  waiting for transfers between devices: 34.5 us -> 0 us
  starting transfers between devices: 19.2 us -> 0 us
  matrix products: 5.8 us -> 0 us
  other arithmetic: 3.71 us -> 0 us
    pallas_call x0 -> x1, Pallas kernels: none -> 79.5 us  [shards(): pl.pallas_call(functools.partial(kernel, n_tp, n_ep), out_shape=(jax.Shap...]
    all_to_all x1 -> x0, blocking collectives: 60.8 us -> none  [shards(): lax.all_to_all(outgoing, 'ep', split_axis=0, concat_axis=2, tiled=True)]
    all_to_all x4 -> x0, waiting for transfers between devices: 34.5 us -> none  [the longest x2 15.6 us: copy_for_each(): return lax.all_to_all(copies, axis, split_axis=0, concat_axis=0, tiled=True)]
    all_to_all x4 -> x0, starting transfers between devices: 19.2 us -> none  [the longest x2 10.9 us: copy_for_each(): return lax.all_to_all(copies, axis, split_axis=0, concat_axis=0, tiled=True)]
    dot_general x12 -> x0, matrix products: 5.8 us -> none  [the longest x1 1.19 us: shards(): jnp.dot(normed, w_query, preferred_element_type=jnp.float32)]
    unnamed x32 -> x3, local copies, waits for them, and re-layouts: 0.23 us -> 3.8 us
    reduce_sum x5 -> x0, other arithmetic: 2.01 us -> none  [the longest x1 0.98 us: shards(): jnp.mean(token_rows * token_rows, axis=1, keepdims=True) + epsilon]
  transfers between devices with their start and end apart: 4 -> 0, of which waited for: 4 -> 0; matrix products, arithmetic and copies ran while one was open for 2% -> 0% of each run, Pallas kernels for 0% -> 0%
where the time goes in v1:
time: 84.9 us; the launch traced here: 84 us
  Pallas kernels  79.5 us (94%)
  local copies, waits for them, and re-layouts  3.8 us (4%)
    pallas_call x1, Pallas kernels, shards(): pl.pallas_call(functools.partial(kernel, n_tp, n_ep), out_shape=(jax.Shap...  79.5 us
    unnamed x3, local copies, waits for them, and re-layouts  3.8 us

profile of v1, /device:TPU:80, one launch (start us, length us, event | category | flops | bytes accessed | tf_op | source)
XLA Modules:
  0.0 84.0 jit_solution(11464324601098738351)
XLA Ops:
  0.6 79.5 %shard_map.175 = (bf16[10,128]{1,0:T(8,128)(2,1)}, bf16[10,64]{1,0:T(8,128)(2,1)}, bf16[10,64]{1,0:T(8,128)(2,1)}) custom-call(bf16[10,1024]{1,0:T(8,128)(2,1)} %tok_hbm.1, f32[1,1024]{1,0:T(1,128)} %bitcast.20, bf16[1024,128]{1,0:T(8,128)(2,1)} %wq_hbm.1, bf16[64,1024]{1,0:T(8,128)(2,1)} %bitcast.18, bf16[64,1024]{1,0:T(8,128)(2,1)} %bitcast.19, ...), custom_call_target="tpu_custom_call" | custom-call | tf_op jit(solution)/shard_map/pallas_call | solution.py:458
  80.2 1.3 %copy.22 = bf16[10,128]{1,0:T(8,128)(2,1)} copy(bf16[10,128]{1,0:T(8,128)(2,1)} %get-tuple-element.6) | data formatting | bytes 5120
  81.4 1.3 %copy.23 = bf16[10,64]{1,0:T(8,128)(2,1)} copy(bf16[10,64]{1,0:T(8,128)(2,1)} %get-tuple-element.7) | data formatting | bytes 2560
  82.7 1.3 %copy.24 = bf16[10,64]{1,0:T(8,128)(2,1)} copy(bf16[10,64]{1,0:T(8,128)(2,1)} %get-tuple-element.8) | data formatting | bytes 2560

commit v2 on v1

--- a/solution.py
+++ b/solution.py
@@ -29,6 +29,10 @@
 
 def near_first(count):
     return sorted(range(1, count), key=lambda step: hops(step, count))
+
+
+def at_part(step, count):
+    return (count - step + count // 4 - 1) % count < count // 2
 
 
 def nt_dot(left, right):
@@ -82,6 +86,7 @@
     hid,
     hg,
     zsend,
+    zrecv,
     xg,
     rsend,
     rrecv,
@@ -108,42 +113,38 @@
     seq_rows = tok.shape[0]
     slots = 2 * n_ep
 
+    def copies_of(first, pairs):
+        made = [
+            pltpu.make_async_copy(source, target, local_sem.at[first + number])
+            for number, (source, target) in enumerate(pairs)
+        ]
+        for copy in made:
+            copy.start()
+        return made
+
+    c_tok, c_again, c_wq, c_len, c_bias, c_key, c_val = copies_of(
+        0,
+        (
+            (tok_hbm, tok),
+            (again_hbm, again),
+            (wq_hbm, wq),
+            (len_hbm, lens),
+            (bias_hbm, bias),
+            (key_hbm, key),
+            (val_hbm, val),
+        ),
+    )
+
+    def wrap(number, count):
+        return jnp.where(number >= count, number - count, number)
+
     barrier = pltpu.get_barrier_semaphore()
     for step in far_first(n_tp):
-        pl.semaphore_signal(barrier, inc=1, device_id={"tp": lax.rem(tp + step, n_tp)})
+        pl.semaphore_signal(barrier, inc=1, device_id={"tp": wrap(tp + step, n_tp)})
 
     @pl.loop(1, n_ep)
     def _(step):
-        pl.semaphore_signal(barrier, inc=1, device_id={"ep": lax.rem(ep + step, n_ep)})
-
-    pairs = (
-        (tok_hbm, tok),
-        (again_hbm, again),
-        (wq_hbm, wq),
-        (len_hbm, lens),
-        (bias_hbm, bias),
-        (key_hbm, key),
-        (ids_hbm, ids),
-        (rw_hbm, rw),
-        (val_hbm, val),
-        (wo_hbm, wo),
-        (fgain_hbm, fgain),
-        (wk_hbm, wk),
-        (wv_hbm, wv),
-        (wg_hbm, wg),
-        (wu_hbm, wu),
-        (wd_hbm, wd),
-    )
-    copies = [
-        pltpu.make_async_copy(source, target, local_sem.at[number])
-        for number, (source, target) in enumerate(pairs)
-    ]
-    for copy in copies:
-        copy.start()
-    (
-        c_tok, c_again, c_wq, c_len, c_bias, c_key, c_ids, c_rw,
-        c_val, c_wo, c_fgain, c_wk, c_wv, c_wg, c_wu, c_wd,
-    ) = copies
+        pl.semaphore_signal(barrier, inc=1, device_id={"ep": wrap(ep + step, n_ep)})
 
     def landed(view, sem):
         pltpu.make_async_copy(view, view, sem).wait()
@@ -184,6 +185,9 @@
     )
 
     c_key.wait()
+    c_wo, c_wk, c_wv, c_ids, c_rw, c_fgain = copies_of(
+        7, ((wo_hbm, wo), (wk_hbm, wk), (wv_hbm, wv), (ids_hbm, ids), (rw_hbm, rw), (fgain_hbm, fgain))
+    )
     scores = jnp.dot(spread, key[...], preferred_element_type=f32) + bias_col
     in_cache = iota(scores.shape, 1).astype(f32) < len_col
     log_rest = -(jnp.maximum(scores, 0.0) + jnp.log1p(jnp.exp(-jnp.abs(scores))))
@@ -216,14 +220,12 @@
     hg[tp] = heads
 
     pl.semaphore_wait(barrier, (n_tp - 1) + (n_ep - 1))
-    sends = []
     for step in far_first(n_tp):
-        copy = pltpu.make_async_remote_copy(
-            hg.at[tp], hg.at[tp], h_ssem.at[step], h_rsem.at[tp], device_id={"tp": lax.rem(tp + step, n_tp)}
-        )
-        copy.start()
-        sends.append(copy)
-
+        pltpu.make_async_remote_copy(
+            hg.at[tp], hg.at[tp], h_ssem, h_rsem, device_id={"tp": wrap(tp + step, n_tp)}
+        ).start()
+
+    c_wg, c_wu, c_wd = copies_of(0, ((wg_hbm, wg), (wu_hbm, wu), (wd_hbm, wd)))
     c_wk.wait()
     c_wv.wait()
     nk_ref[...] = nt_dot(normed, wk[...]).astype(bf16)
@@ -252,77 +254,55 @@
     own_gain = fgain[:, own_cols]
 
     c_wo.wait()
-    attn_out = jnp.dot(hg[tp], wo[own_cols, :], preferred_element_type=f32)
-    for step in near_first(n_tp):
-        peer = lax.rem(tp + step, n_tp)
-        landed(hg.at[peer], h_rsem.at[peer])
-        attn_out += jnp.dot(
-            hg[peer], wo[pl.ds(pl.multiple_of(peer * LANES, LANES), LANES), :], preferred_element_type=f32
-        )
+    inverse_sq = 1.0 / (fgain[...] * fgain[...])
+    peers = pl.ds(0, n_tp - 1)
+    landed(hg.at[peers], h_rsem)
+    all_heads = jnp.concatenate([hg[peer] for peer in range(n_tp)], axis=1)
+    attn_out = jnp.dot(all_heads, wo[...], preferred_element_type=f32)
     hid[pl.ds(0, seq_rows), :] = own_tokens + attn_out[:seq_rows]
     scaled = (hid[...] * own_gain).astype(bf16)
     outgoing = jnp.dot(place[...], scaled, preferred_element_type=f32).astype(bf16)
     zsend[...] = outgoing.reshape(zsend.shape)
 
-    for step in far_first(chips):
-        for to_core in range(CORES):
-            to_ep = lax.rem(chip + step, chips) * CORES + to_core
-            at = ((chips - step + chips // 4 - 1) % chips) * CORES + core
-            copy = pltpu.make_async_remote_copy(
-                zsend.at[to_ep],
-                xg.at[tp, at],
-                z_ssem.at[step * CORES + to_core],
-                z_rsem.at[at],
-                device_id={"ep": to_ep},
-            )
-            copy.start()
-            sends.append(copy)
     home = (chips // 4 - 1) * CORES
     partner = chip * CORES + (1 - core)
-    copy = pltpu.make_async_remote_copy(
-        zsend.at[partner], xg.at[tp, home + core], z_ssem.at[0], z_rsem.at[home + core], device_id={"ep": partner}
-    )
-    copy.start()
-    sends.append(copy)
-    xg[tp, home + core] = zsend[ep]
+    for step in far_first(chips) + [0]:
+        to_chip = wrap(chip + step, chips)
+        at = ((chips - step + chips // 4 - 1) % chips) * CORES + core
+        part = 0 if at_part(step, chips) else 1
+        for to_core in range(CORES):
+            to_ep = to_chip * CORES + to_core if step else partner
+            if step == 0 and to_core:
+                continue
+            pltpu.make_async_remote_copy(
+                zsend.at[to_ep], zrecv.at[at], z_ssem, z_rsem.at[part], device_id={"ep": to_ep}
+            ).start()
+    zrecv[home + core] = zsend[ep]
 
     for part in range(2):
-        for number in range(half):
-            at = part * half + number
-            if at // CORES == home // CORES:
-                continue
-            landed(xg.at[tp, at], z_rsem.at[at])
-        if part == 0:
-            landed(xg.at[tp, home + 1 - core], z_rsem.at[home + 1 - core])
-        span_at = pl.ds(part * half, half)
+        landed(zrecv.at[pl.ds(part * half, half - 1 + part)], z_rsem.at[part])
+        xg[part, tp] = zrecv[pl.ds(part * half, half)].reshape(slots // 2, LANES)
         for step in far_first(n_tp):
-            copy = pltpu.make_async_remote_copy(
-                xg.at[tp, span_at],
-                xg.at[tp, span_at],
-                g_ssem.at[part, step],
-                g_rsem.at[part, tp],
-                device_id={"tp": lax.rem(tp + step, n_tp)},
-            )
-            copy.start()
-            sends.append(copy)
+            pltpu.make_async_remote_copy(
+                xg.at[part, tp],
+                xg.at[part, tp],
+                g_ssem.at[part],
+                g_rsem.at[part],
+                device_id={"tp": wrap(tp + step, n_tp)},
+            ).start()
 
     c_wg.wait()
     c_wu.wait()
     c_wd.wait()
-    gate = jnp.zeros((slots, wg.shape[1]), f32)
-    up = jnp.zeros((slots, wu.shape[1]), f32)
-    sum_sq = jnp.zeros((slots, 1), f32)
-    for step in [0] + near_first(n_tp):
-        peer = lax.rem(tp + step, n_tp)
-        if step:
-            for part in range(2):
-                landed(xg.at[peer, pl.ds(part * half, half)], g_rsem.at[part, peer])
-        rows = xg[peer].reshape(slots, LANES)
-        peer_cols = pl.ds(pl.multiple_of(peer * LANES, LANES), LANES)
-        gate += jnp.dot(rows, wg[peer_cols, :], preferred_element_type=f32)
-        up += jnp.dot(rows, wu[peer_cols, :], preferred_element_type=f32)
-        plain = rows.astype(f32) / fgain[:, peer_cols]
-        sum_sq += jnp.sum(plain * plain, axis=1, keepdims=True)
+    for part in range(2):
+        landed(xg.at[part, peers], g_rsem.at[part])
+    rows = jnp.concatenate(
+        [jnp.concatenate([xg[part, peer] for peer in range(n_tp)], axis=1) for part in range(2)], axis=0
+    )
+    gate = jnp.dot(rows, wg[...], preferred_element_type=f32)
+    up = jnp.dot(rows, wu[...], preferred_element_type=f32)
+    plain = rows.astype(f32)
+    sum_sq = jnp.sum(plain * plain * inverse_sq, axis=1, keepdims=True)
     scale = lax.rsqrt(sum_sq / (n_tp * LANES) + epsilon)
     gate = gate * scale
     up = up * scale
@@ -333,55 +313,51 @@
         for c in range(n_tp):
             rsend[part, c] = partial_value[:, c * LANES : (c + 1) * LANES]
         for step in far_first(n_tp):
-            peer = lax.rem(tp + step, n_tp)
-            copy = pltpu.make_async_remote_copy(
-                rsend.at[part, peer],
-                rrecv.at[part, tp],
-                r_ssem.at[part, step],
-                r_rsem.at[part, tp],
-                device_id={"tp": peer},
-            )
-            copy.start()
-            sends.append(copy)
+            peer = wrap(tp + step, n_tp)
+            pltpu.make_async_remote_copy(
+                rsend.at[part, peer], rrecv.at[part, tp], r_ssem.at[part], r_rsem.at[part], device_id={"tp": peer}
+            ).start()
+        rrecv[part, tp] = rsend[part, tp]
 
     for part in (1, 0):
-        total = rsend[part, tp].astype(f32)
-        for step in near_first(n_tp):
-            peer = lax.rem(tp + step, n_tp)
-            landed(rrecv.at[part, peer], r_rsem.at[part, peer])
+        landed(rrecv.at[part, peers], r_rsem.at[part])
+        total = rrecv[part, 0].astype(f32)
+        for peer in range(1, n_tp):
             total += rrecv[part, peer].astype(f32)
-        span_at = pl.ds(part * half, half)
-        ysend[span_at] = total.astype(bf16).reshape(half, 2, LANES)
+        ysend[pl.ds(part * half, half)] = total.astype(bf16).reshape(half, 2, LANES)
         order = range(half * part, half * (part + 1))
-        order = sorted(order, key=lambda at: -hops((at - home) // CORES, chips))
-        for at in order:
+        for at in sorted(order, key=lambda at: -hops((at - home) // CORES, chips)):
             step = at // CORES - home // CORES
-            if step == 0:
-                continue
-            to_ep = lax.rem(chip + step + chips, chips) * CORES + at % CORES
-            copy = pltpu.make_async_remote_copy(
-                ysend.at[at], ret.at[ep], y_ssem.at[at], y_rsem.at[ep], device_id={"ep": to_ep}
-            )
-            copy.start()
-            sends.append(copy)
+            if step:
+                to_ep = wrap(chip + step % chips, chips) * CORES + at % CORES
+                pltpu.make_async_remote_copy(
+                    ysend.at[at], ret.at[ep], y_ssem, y_rsem, device_id={"ep": to_ep}
+                ).start()
         if part == 0:
-            copy = pltpu.make_async_remote_copy(
-                ysend.at[home + 1 - core], ret.at[ep], y_ssem.at[home], y_rsem.at[ep], device_id={"ep": partner}
-            )
-            copy.start()
-            sends.append(copy)
+            pltpu.make_async_remote_copy(
+                ysend.at[home + 1 - core], ret.at[ep], y_ssem, y_rsem, device_id={"ep": partner}
+            ).start()
             ret[ep] = ysend[home + core]
 
-    for step in near_first(chips):
-        for from_core in range(CORES):
-            from_ep = lax.rem(chip + step, chips) * CORES + from_core
-            landed(ret.at[from_ep], y_rsem.at[from_ep])
-    landed(ret.at[partner], y_rsem.at[partner])
+    landed(hg.at[peers], h_ssem)
+    landed(zsend.at[pl.ds(0, n_ep - 1)], z_ssem)
+    for part in range(2):
+        landed(xg.at[part, peers], g_ssem.at[part])
+        landed(rsend.at[part, peers], r_ssem.at[part])
+    landed(ysend.at[pl.ds(0, n_ep - 1)], y_ssem)
+    landed(ret.at[pl.ds(0, n_ep - 1)], y_rsem)
     picked = jnp.dot(combine[...], ret[...].reshape(slots, LANES), preferred_element_type=f32)
     routed_sum = picked[:pad_rows] + picked[pad_rows:]
     mixed_ref[...] = (hid[pl.ds(0, seq_rows), :] + routed_sum[:seq_rows]).astype(bf16)
-    for copy in sends:
-        copy.wait_send()
+
+
+def write_out(*refs):
+    count = len(refs) // 2
+    copies = [pltpu.make_async_copy(refs[n], refs[count + n], refs[-1].at[n]) for n in range(count)]
+    for copy in copies:
+        copy.start()
+    for copy in copies:
+        copy.wait()
 
 
 def shards(
@@ -438,35 +414,44 @@
         pltpu.VMEM((LANES, LANES), f32),
         pltpu.VMEM((n_tp, pad_rows, LANES), bf16),
         pltpu.VMEM((n_ep, 2, LANES), bf16),
-        pltpu.VMEM((n_tp, n_ep, 2, LANES), bf16),
+        pltpu.VMEM((n_ep, 2, LANES), bf16),
+        pltpu.VMEM((2, n_tp, slots // 2, LANES), bf16),
         pltpu.VMEM((2, n_tp, slots // 2, LANES), bf16),
         pltpu.VMEM((2, n_tp, slots // 2, LANES), bf16),
         pltpu.VMEM((n_ep, 2, LANES), bf16),
         pltpu.VMEM((n_ep, 2, LANES), bf16),
-        dma((len(operands),)),
-        dma((n_tp,)),
-        dma((n_tp,)),
-        dma((n_ep,)),
-        dma((n_ep,)),
-        dma((2, n_tp)),
-        dma((2, n_tp)),
-        dma((2, n_tp)),
-        dma((2, n_tp)),
-        dma((n_ep,)),
-        dma((n_ep,)),
+        dma((13,)),
+        dma,
+        dma,
+        dma,
+        dma((2,)),
+        dma((2,)),
+        dma((2,)),
+        dma((2,)),
+        dma((2,)),
+        dma,
+        dma,
     ]
-    return pl.pallas_call(
+    shapes = (
+        (seq_rows, w_out.shape[1]),
+        (seq_rows, w_key.shape[1]),
+        (seq_rows, w_value.shape[1]),
+    )
+    results = pl.pallas_call(
         functools.partial(kernel, n_tp, n_ep),
-        out_shape=(
-            jax.ShapeDtypeStruct((seq_rows, w_out.shape[1]), bf16),
-            jax.ShapeDtypeStruct((seq_rows, w_key.shape[1]), bf16),
-            jax.ShapeDtypeStruct((seq_rows, w_value.shape[1]), bf16),
-        ),
+        out_shape=tuple(pltpu.VMEM(shape, bf16) for shape in shapes),
         in_specs=[pl.BlockSpec(memory_space=pltpu.HBM)] * len(operands),
         out_specs=[pl.BlockSpec(memory_space=pltpu.VMEM)] * 3,
         scratch_shapes=scratch,
         compiler_params=pltpu.CompilerParams(collective_id=0, has_side_effects=True),
     )(*operands)
+    return pl.pallas_call(
+        write_out,
+        out_shape=tuple(jax.ShapeDtypeStruct(shape, bf16) for shape in shapes),
+        in_specs=[pl.BlockSpec(memory_space=pltpu.VMEM)] * 3,
+        out_specs=[pl.BlockSpec(memory_space=pltpu.HBM)] * 3,
+        scratch_shapes=[dma((3,))],
+    )(*[pltpu.with_memory_space_constraint(r, pltpu.VMEM) for r in results])
 
 
 def solution(mesh):

time: 84.9 us -> 79.3 us (0.934)
  local copies, waits for them, and re-layouts: 3.8 us -> 0 us
  Pallas kernels: 79.5 us -> 77.7 us
    unnamed x3 -> x0, local copies, waits for them, and re-layouts: 3.8 us -> none
    pallas_call x1 -> x2, Pallas kernels: 79.5 us -> 77.7 us  [the longest x1 77.1 us: shards(): pl.pallas_call(functools.partial(kernel, n_tp, n_ep), out_shape=tuple((pl...]
where the time goes in v2:
time: 79.3 us; the launch traced here: 78.4 us
  Pallas kernels  77.7 us (98%)
    pallas_call x1, Pallas kernels, shards(): pl.pallas_call(functools.partial(kernel, n_tp, n_ep), out_shape=tuple((pl...  77.1 us

profile of v2, /device:TPU:80, one launch (start us, length us, event | category | flops | bytes accessed | tf_op | source)
XLA Modules:
  0.0 78.4 jit_solution(4204249167019623420)
XLA Ops:
  0.6 77.1 %shard_map.175 = (bf16[10,128]{1,0:T(8,128)(2,1)S(1)}, bf16[10,64]{1,0:T(8,128)(2,1)S(1)}, bf16[10,64]{1,0:T(8,128)(2,1)S(1)}) custom-call(bf16[10,1024]{1,0:T(8,128)(2,1)} %tok_hbm.1, f32[1,1024]{1,0:T(1,128)} %bitcast.20, bf16[1024,128]{1,0:T(8,128)(2,1)} %wq_hbm.1, bf16[64,1024]{1,0:T(8,128)(2,1)} %bitcast.18, bf16[64,1024]{1,0:T(8,128)(2,1)} %bitcast.19, ...), custom_call_target="tpu_custom_call" | custom-call | tf_op jit(solution)/shard_map/pallas_call | solution.py:440
  77.8 0.6 shard_map.176

commit v3 on v2

--- a/solution.py
+++ b/solution.py
@@ -29,10 +29,6 @@
 
 def near_first(count):
     return sorted(range(1, count), key=lambda step: hops(step, count))
-
-
-def at_part(step, count):
-    return (count - step + count // 4 - 1) % count < count // 2
 
 
 def nt_dot(left, right):
@@ -264,24 +260,27 @@
     outgoing = jnp.dot(place[...], scaled, preferred_element_type=f32).astype(bf16)
     zsend[...] = outgoing.reshape(zsend.shape)
 
-    home = (chips // 4 - 1) * CORES
+    own_part = ep // half
+    for step in far_first(chips):
+        to_chip = wrap(chip + step, chips)
+        for to_core in range(CORES):
+            to_ep = to_chip * CORES + to_core
+            pltpu.make_async_remote_copy(
+                zsend.at[to_ep], zrecv.at[ep], z_ssem, z_rsem.at[own_part], device_id={"ep": to_ep}
+            ).start()
     partner = chip * CORES + (1 - core)
-    for step in far_first(chips) + [0]:
-        to_chip = wrap(chip + step, chips)
-        at = ((chips - step + chips // 4 - 1) % chips) * CORES + core
-        part = 0 if at_part(step, chips) else 1
-        for to_core in range(CORES):
-            to_ep = to_chip * CORES + to_core if step else partner
-            if step == 0 and to_core:
-                continue
-            pltpu.make_async_remote_copy(
-                zsend.at[to_ep], zrecv.at[at], z_ssem, z_rsem.at[part], device_id={"ep": to_ep}
-            ).start()
-    zrecv[home + core] = zsend[ep]
-
+    pltpu.make_async_remote_copy(
+        zsend.at[partner], zrecv.at[ep], z_ssem, z_rsem.at[own_part], device_id={"ep": partner}
+    ).start()
+    pltpu.make_async_copy(zsend.at[ep], zrecv.at[ep], z_rsem.at[own_part]).start()
+
+    c_wg.wait()
+    c_wu.wait()
+    c_wd.wait()
     for part in range(2):
-        landed(zrecv.at[pl.ds(part * half, half - 1 + part)], z_rsem.at[part])
-        xg[part, tp] = zrecv[pl.ds(part * half, half)].reshape(slots // 2, LANES)
+        span_at = pl.ds(part * half, half)
+        landed(zrecv.at[span_at], z_rsem.at[part])
+        xg[part, tp] = zrecv[span_at].reshape(slots // 2, LANES)
         for step in far_first(n_tp):
             pltpu.make_async_remote_copy(
                 xg.at[part, tp],
@@ -290,26 +289,17 @@
                 g_rsem.at[part],
                 device_id={"tp": wrap(tp + step, n_tp)},
             ).start()
-
-    c_wg.wait()
-    c_wu.wait()
-    c_wd.wait()
-    for part in range(2):
         landed(xg.at[part, peers], g_rsem.at[part])
-    rows = jnp.concatenate(
-        [jnp.concatenate([xg[part, peer] for peer in range(n_tp)], axis=1) for part in range(2)], axis=0
-    )
-    gate = jnp.dot(rows, wg[...], preferred_element_type=f32)
-    up = jnp.dot(rows, wu[...], preferred_element_type=f32)
-    plain = rows.astype(f32)
-    sum_sq = jnp.sum(plain * plain * inverse_sq, axis=1, keepdims=True)
-    scale = lax.rsqrt(sum_sq / (n_tp * LANES) + epsilon)
-    gate = gate * scale
-    up = up * scale
-    hidden_act = (gate / (1.0 + jnp.exp(-gate)) * up).astype(bf16)
-    for part in (1, 0):
-        act = hidden_act[part * slots // 2 : (part + 1) * slots // 2]
-        partial_value = jnp.dot(act, wd[...], preferred_element_type=f32).astype(bf16)
+        rows = jnp.concatenate([xg[part, peer] for peer in range(n_tp)], axis=1)
+        gate = jnp.dot(rows, wg[...], preferred_element_type=f32)
+        up = jnp.dot(rows, wu[...], preferred_element_type=f32)
+        plain = rows.astype(f32)
+        sum_sq = jnp.sum(plain * plain * inverse_sq, axis=1, keepdims=True)
+        scale = lax.rsqrt(sum_sq / (n_tp * LANES) + epsilon)
+        gate = gate * scale
+        up = up * scale
+        hidden_act = (gate / (1.0 + jnp.exp(-gate)) * up).astype(bf16)
+        partial_value = jnp.dot(hidden_act, wd[...], preferred_element_type=f32).astype(bf16)
         for c in range(n_tp):
             rsend[part, c] = partial_value[:, c * LANES : (c + 1) * LANES]
         for step in far_first(n_tp):
@@ -318,34 +308,27 @@
                 rsend.at[part, peer], rrecv.at[part, tp], r_ssem.at[part], r_rsem.at[part], device_id={"tp": peer}
             ).start()
         rrecv[part, tp] = rsend[part, tp]
-
-    for part in (1, 0):
         landed(rrecv.at[part, peers], r_rsem.at[part])
         total = rrecv[part, 0].astype(f32)
         for peer in range(1, n_tp):
             total += rrecv[part, peer].astype(f32)
-        ysend[pl.ds(part * half, half)] = total.astype(bf16).reshape(half, 2, LANES)
-        order = range(half * part, half * (part + 1))
-        for at in sorted(order, key=lambda at: -hops((at - home) // CORES, chips)):
-            step = at // CORES - home // CORES
-            if step:
-                to_ep = wrap(chip + step % chips, chips) * CORES + at % CORES
+        ysend[span_at] = total.astype(bf16).reshape(half, 2, LANES)
+        for to_ep in range(half * part, half * (part + 1)):
+
+            @pl.when(to_ep != ep)
+            def _():
                 pltpu.make_async_remote_copy(
-                    ysend.at[at], ret.at[ep], y_ssem, y_rsem, device_id={"ep": to_ep}
+                    ysend.at[to_ep], ret.at[ep], y_ssem, y_rsem, device_id={"ep": to_ep}
                 ).start()
-        if part == 0:
-            pltpu.make_async_remote_copy(
-                ysend.at[home + 1 - core], ret.at[ep], y_ssem, y_rsem, device_id={"ep": partner}
-            ).start()
-            ret[ep] = ysend[home + core]
-
+
+    pltpu.make_async_copy(ysend.at[ep], ret.at[ep], y_rsem).start()
     landed(hg.at[peers], h_ssem)
     landed(zsend.at[pl.ds(0, n_ep - 1)], z_ssem)
     for part in range(2):
         landed(xg.at[part, peers], g_ssem.at[part])
         landed(rsend.at[part, peers], r_ssem.at[part])
     landed(ysend.at[pl.ds(0, n_ep - 1)], y_ssem)
-    landed(ret.at[pl.ds(0, n_ep - 1)], y_rsem)
+    landed(ret, y_rsem)
     picked = jnp.dot(combine[...], ret[...].reshape(slots, LANES), preferred_element_type=f32)
     routed_sum = picked[:pad_rows] + picked[pad_rows:]
     mixed_ref[...] = (hid[pl.ds(0, seq_rows), :] + routed_sum[:seq_rows]).astype(bf16)

time: 79.3 us -> 84.4 us (1.064)
  Pallas kernels: 77.7 us -> 83.6 us
    pallas_call x1, Pallas kernels: 77.1 us -> 82.9 us  [shards(): pl.pallas_call(functools.partial(kernel, n_tp, n_ep), out_shape=tuple((pl...]
where the time goes in v3:
time: 84.4 us; the launch traced here: 84.2 us
  Pallas kernels  83.6 us (99%)
    pallas_call x1, Pallas kernels, shards(): pl.pallas_call(functools.partial(kernel, n_tp, n_ep), out_shape=tuple((pl...  82.9 us

profile of v3, /device:TPU:80, one launch (start us, length us, event | category | flops | bytes accessed | tf_op | source)
XLA Modules:
  0.0 84.2 jit_solution(10663392056298545013)
XLA Ops:
  0.6 82.9 %shard_map.175 = (bf16[10,128]{1,0:T(8,128)(2,1)S(1)}, bf16[10,64]{1,0:T(8,128)(2,1)S(1)}, bf16[10,64]{1,0:T(8,128)(2,1)S(1)}) custom-call(bf16[10,1024]{1,0:T(8,128)(2,1)} %tok_hbm.1, f32[1,1024]{1,0:T(1,128)} %bitcast.20, bf16[1024,128]{1,0:T(8,128)(2,1)} %wq_hbm.1, bf16[64,1024]{1,0:T(8,128)(2,1)} %bitcast.18, bf16[64,1024]{1,0:T(8,128)(2,1)} %bitcast.19, ...), custom_call_target="tpu_custom_call" | custom-call | tf_op jit(solution)/shard_map/pallas_call | solution.py:423
  83.6 0.6 shard_map.176

commit v4 on v3

--- a/solution.py
+++ b/solution.py
@@ -99,13 +99,13 @@
     r_rsem,
     y_ssem,
     y_rsem,
+    ready,
 ):
     tp = lax.axis_index("tp")
     ep = lax.axis_index("ep")
     core = lax.rem(ep, CORES)
     chip = ep // CORES
     chips = n_ep // CORES
-    half = n_ep // 2
     seq_rows = tok.shape[0]
     slots = 2 * n_ep
 
@@ -135,12 +135,19 @@
         return jnp.where(number >= count, number - count, number)
 
     barrier = pltpu.get_barrier_semaphore()
+    column = tp == 0
+    topmost = jnp.logical_and(column, ep == 0)
+    partner = chip * CORES + (1 - core)
     for step in far_first(n_tp):
         pl.semaphore_signal(barrier, inc=1, device_id={"tp": wrap(tp + step, n_tp)})
 
-    @pl.loop(1, n_ep)
-    def _(step):
-        pl.semaphore_signal(barrier, inc=1, device_id={"ep": wrap(ep + step, n_ep)})
+    @pl.loop(jnp.where(topmost, n_ep, ep + 1), n_ep)
+    def _(above):
+        pl.semaphore_signal(barrier, inc=1, device_id={"ep": above})
+
+    @pl.when(jnp.logical_and(column, ep > 0))
+    def _():
+        pl.semaphore_signal(barrier, inc=1, device_id={"ep": 0})
 
     def landed(view, sem):
         pltpu.make_async_copy(view, view, sem).wait()
@@ -215,11 +222,16 @@
     heads = jnp.where(low, folded[:pad_rows], folded[pad_rows:]).astype(bf16)
     hg[tp] = heads
 
-    pl.semaphore_wait(barrier, (n_tp - 1) + (n_ep - 1))
+    lowest = jnp.where(column, 1, 0)
+    pl.semaphore_wait(barrier, (n_tp - 1) + jnp.where(topmost, n_ep - 1, ep - lowest))
     for step in far_first(n_tp):
         pltpu.make_async_remote_copy(
             hg.at[tp], hg.at[tp], h_ssem, h_rsem, device_id={"tp": wrap(tp + step, n_tp)}
         ).start()
+
+    @pl.loop(lowest, jnp.where(topmost, n_ep, ep))
+    def _(below):
+        pl.semaphore_signal(ready.at[chip], inc=1, device_id={"ep": below})
 
     c_wg, c_wu, c_wd = copies_of(0, ((wg_hbm, wg), (wu_hbm, wu), (wd_hbm, wd)))
     c_wk.wait()
@@ -260,37 +272,54 @@
     outgoing = jnp.dot(place[...], scaled, preferred_element_type=f32).astype(bf16)
     zsend[...] = outgoing.reshape(zsend.shape)
 
-    own_part = ep // half
-    for step in far_first(chips):
-        to_chip = wrap(chip + step, chips)
-        for to_core in range(CORES):
-            to_ep = to_chip * CORES + to_core
+    bounds = (0, n_ep // 4, n_ep)
+    own_group = jnp.where(ep >= bounds[1], 1, 0)
+    def send_slots(to_ep):
+        @pl.when(to_ep != ep)
+        def _():
             pltpu.make_async_remote_copy(
-                zsend.at[to_ep], zrecv.at[ep], z_ssem, z_rsem.at[own_part], device_id={"ep": to_ep}
+                zsend.at[to_ep], zrecv.at[ep], z_ssem, z_rsem.at[own_group], device_id={"ep": to_ep}
             ).start()
-    partner = chip * CORES + (1 - core)
-    pltpu.make_async_remote_copy(
-        zsend.at[partner], zrecv.at[ep], z_ssem, z_rsem.at[own_part], device_id={"ep": partner}
-    ).start()
-    pltpu.make_async_copy(zsend.at[ep], zrecv.at[ep], z_rsem.at[own_part]).start()
+
+    for to_chip in range(chips):
+
+        @pl.when(jnp.logical_and(to_chip > chip, jnp.logical_not(topmost)))
+        def _():
+            pl.semaphore_wait(ready.at[to_chip], CORES)
+
+        @pl.when(jnp.logical_and(jnp.logical_and(to_chip == chip, core == 0), jnp.logical_not(topmost)))
+        def _():
+            pl.semaphore_wait(ready.at[to_chip], 1)
+
+        for to_ep in range(max(1, to_chip * CORES), (to_chip + 1) * CORES):
+            send_slots(to_ep)
+
+    @pl.when(jnp.logical_and(column, ep > 0))
+    def _():
+        pl.semaphore_wait(ready.at[0], 1)
+
+    send_slots(0)
+    pltpu.make_async_copy(zsend.at[ep], zrecv.at[ep], z_rsem.at[own_group]).start()
 
     c_wg.wait()
     c_wu.wait()
     c_wd.wait()
-    for part in range(2):
-        span_at = pl.ds(part * half, half)
-        landed(zrecv.at[span_at], z_rsem.at[part])
-        xg[part, tp] = zrecv[span_at].reshape(slots // 2, LANES)
+    for group, (first, last) in enumerate(zip(bounds[:-1], bounds[1:])):
+        count = last - first
+        eps = pl.ds(first, count)
+        here = pl.ds(2 * first, 2 * count)
+        landed(zrecv.at[eps], z_rsem.at[group])
+        xg[tp, here] = zrecv[eps].reshape(2 * count, LANES)
         for step in far_first(n_tp):
             pltpu.make_async_remote_copy(
-                xg.at[part, tp],
-                xg.at[part, tp],
-                g_ssem.at[part],
-                g_rsem.at[part],
+                xg.at[tp, here],
+                xg.at[tp, here],
+                g_ssem.at[group],
+                g_rsem.at[group],
                 device_id={"tp": wrap(tp + step, n_tp)},
             ).start()
-        landed(xg.at[part, peers], g_rsem.at[part])
-        rows = jnp.concatenate([xg[part, peer] for peer in range(n_tp)], axis=1)
+        landed(xg.at[peers, here], g_rsem.at[group])
+        rows = jnp.concatenate([xg[peer, here] for peer in range(n_tp)], axis=1)
         gate = jnp.dot(rows, wg[...], preferred_element_type=f32)
         up = jnp.dot(rows, wu[...], preferred_element_type=f32)
         plain = rows.astype(f32)
@@ -301,19 +330,19 @@
         hidden_act = (gate / (1.0 + jnp.exp(-gate)) * up).astype(bf16)
         partial_value = jnp.dot(hidden_act, wd[...], preferred_element_type=f32).astype(bf16)
         for c in range(n_tp):
-            rsend[part, c] = partial_value[:, c * LANES : (c + 1) * LANES]
+            rsend[c, here] = partial_value[:, c * LANES : (c + 1) * LANES]
         for step in far_first(n_tp):
             peer = wrap(tp + step, n_tp)
             pltpu.make_async_remote_copy(
-                rsend.at[part, peer], rrecv.at[part, tp], r_ssem.at[part], r_rsem.at[part], device_id={"tp": peer}
+                rsend.at[peer, here], rrecv.at[tp, here], r_ssem.at[group], r_rsem.at[group], device_id={"tp": peer}
             ).start()
-        rrecv[part, tp] = rsend[part, tp]
-        landed(rrecv.at[part, peers], r_rsem.at[part])
-        total = rrecv[part, 0].astype(f32)
+        rrecv[tp, here] = rsend[tp, here]
+        landed(rrecv.at[peers, here], r_rsem.at[group])
+        total = rrecv[0, here].astype(f32)
         for peer in range(1, n_tp):
-            total += rrecv[part, peer].astype(f32)
-        ysend[span_at] = total.astype(bf16).reshape(half, 2, LANES)
-        for to_ep in range(half * part, half * (part + 1)):
+            total += rrecv[peer, here].astype(f32)
+        ysend[eps] = total.astype(bf16).reshape(count, 2, LANES)
+        for to_ep in range(first, last):
 
             @pl.when(to_ep != ep)
             def _():
@@ -324,9 +353,10 @@
     pltpu.make_async_copy(ysend.at[ep], ret.at[ep], y_rsem).start()
     landed(hg.at[peers], h_ssem)
     landed(zsend.at[pl.ds(0, n_ep - 1)], z_ssem)
-    for part in range(2):
-        landed(xg.at[part, peers], g_ssem.at[part])
-        landed(rsend.at[part, peers], r_ssem.at[part])
+    for group, (first, last) in enumerate(zip(bounds[:-1], bounds[1:])):
+        here = pl.ds(2 * first, 2 * (last - first))
+        landed(xg.at[peers, here], g_ssem.at[group])
+        landed(rsend.at[peers, here], r_ssem.at[group])
     landed(ysend.at[pl.ds(0, n_ep - 1)], y_ssem)
     landed(ret, y_rsem)
     picked = jnp.dot(combine[...], ret[...].reshape(slots, LANES), preferred_element_type=f32)
@@ -398,9 +428,9 @@
         pltpu.VMEM((n_tp, pad_rows, LANES), bf16),
         pltpu.VMEM((n_ep, 2, LANES), bf16),
         pltpu.VMEM((n_ep, 2, LANES), bf16),
-        pltpu.VMEM((2, n_tp, slots // 2, LANES), bf16),
-        pltpu.VMEM((2, n_tp, slots // 2, LANES), bf16),
-        pltpu.VMEM((2, n_tp, slots // 2, LANES), bf16),
+        pltpu.VMEM((n_tp, slots, LANES), bf16),
+        pltpu.VMEM((n_tp, slots, LANES), bf16),
+        pltpu.VMEM((n_tp, slots, LANES), bf16),
         pltpu.VMEM((n_ep, 2, LANES), bf16),
         pltpu.VMEM((n_ep, 2, LANES), bf16),
         dma((13,)),
@@ -414,6 +444,7 @@
         dma((2,)),
         dma,
         dma,
+        pltpu.SemaphoreType.REGULAR((n_ep // CORES,)),
     ]
     shapes = (
         (seq_rows, w_out.shape[1]),

time: 84.4 us -> 77 us (0.912)
  Pallas kernels: 83.6 us -> 76.2 us
    pallas_call x1, Pallas kernels: 82.9 us -> 75.6 us  [shards(): pl.pallas_call(functools.partial(kernel, n_tp, n_ep), out_shape=tuple((pl...]
where the time goes in v4:
time: 77 us; the launch traced here: 76.9 us
  Pallas kernels  76.2 us (99%)
    pallas_call x1, Pallas kernels, shards(): pl.pallas_call(functools.partial(kernel, n_tp, n_ep), out_shape=tuple((pl...  75.6 us

profile of v4, /device:TPU:80, one launch (start us, length us, event | category | flops | bytes accessed | tf_op | source)
XLA Modules:
  0.0 76.9 jit_solution(15222401179557352366)
XLA Ops:
  0.6 75.6 %shard_map.175 = (bf16[10,128]{1,0:T(8,128)(2,1)S(1)}, bf16[10,64]{1,0:T(8,128)(2,1)S(1)}, bf16[10,64]{1,0:T(8,128)(2,1)S(1)}) custom-call(bf16[10,1024]{1,0:T(8,128)(2,1)} %tok_hbm.1, f32[1,1024]{1,0:T(1,128)} %bitcast.20, bf16[1024,128]{1,0:T(8,128)(2,1)} %wq_hbm.1, bf16[64,1024]{1,0:T(8,128)(2,1)} %bitcast.18, bf16[64,1024]{1,0:T(8,128)(2,1)} %bitcast.19, ...), custom_call_target="tpu_custom_call" | custom-call | tf_op jit(solution)/shard_map/pallas_call | solution.py:454
  76.2 0.6 shard_map.176

commit v5 on v4

--- a/solution.py
+++ b/solution.py
@@ -281,7 +281,17 @@
                 zsend.at[to_ep], zrecv.at[ep], z_ssem, z_rsem.at[own_group], device_id={"ep": to_ep}
             ).start()
 
+    @pl.when(jnp.logical_not(column))
+    def _():
+        send_slots(0)
+
     for to_chip in range(chips):
+        if to_chip == chips - 1:
+
+            @pl.when(jnp.logical_and(column, ep > 0))
+            def _():
+                pl.semaphore_wait(ready.at[0], 1)
+                send_slots(0)
 
         @pl.when(jnp.logical_and(to_chip > chip, jnp.logical_not(topmost)))
         def _():
@@ -294,22 +304,18 @@
         for to_ep in range(max(1, to_chip * CORES), (to_chip + 1) * CORES):
             send_slots(to_ep)
 
-    @pl.when(jnp.logical_and(column, ep > 0))
-    def _():
-        pl.semaphore_wait(ready.at[0], 1)
-
-    send_slots(0)
     pltpu.make_async_copy(zsend.at[ep], zrecv.at[ep], z_rsem.at[own_group]).start()
 
     c_wg.wait()
     c_wu.wait()
     c_wd.wait()
-    for group, (first, last) in enumerate(zip(bounds[:-1], bounds[1:])):
-        count = last - first
-        eps = pl.ds(first, count)
-        here = pl.ds(2 * first, 2 * count)
+    groups = tuple(zip(bounds[:-1], bounds[1:]))
+
+    def gather(group):
+        first, last = groups[group]
+        eps, here = pl.ds(first, last - first), pl.ds(2 * first, 2 * (last - first))
         landed(zrecv.at[eps], z_rsem.at[group])
-        xg[tp, here] = zrecv[eps].reshape(2 * count, LANES)
+        xg[tp, here] = zrecv[eps].reshape(2 * (last - first), LANES)
         for step in far_first(n_tp):
             pltpu.make_async_remote_copy(
                 xg.at[tp, here],
@@ -318,6 +324,10 @@
                 g_rsem.at[group],
                 device_id={"tp": wrap(tp + step, n_tp)},
             ).start()
+
+    def experts(group):
+        first, last = groups[group]
+        here = pl.ds(2 * first, 2 * (last - first))
         landed(xg.at[peers, here], g_rsem.at[group])
         rows = jnp.concatenate([xg[peer, here] for peer in range(n_tp)], axis=1)
         gate = jnp.dot(rows, wg[...], preferred_element_type=f32)
@@ -337,11 +347,15 @@
                 rsend.at[peer, here], rrecv.at[tp, here], r_ssem.at[group], r_rsem.at[group], device_id={"tp": peer}
             ).start()
         rrecv[tp, here] = rsend[tp, here]
+
+    def give_back(group):
+        first, last = groups[group]
+        eps, here = pl.ds(first, last - first), pl.ds(2 * first, 2 * (last - first))
         landed(rrecv.at[peers, here], r_rsem.at[group])
         total = rrecv[0, here].astype(f32)
         for peer in range(1, n_tp):
             total += rrecv[peer, here].astype(f32)
-        ysend[eps] = total.astype(bf16).reshape(count, 2, LANES)
+        ysend[eps] = total.astype(bf16).reshape(last - first, 2, LANES)
         for to_ep in range(first, last):
 
             @pl.when(to_ep != ep)
@@ -350,18 +364,24 @@
                     ysend.at[to_ep], ret.at[ep], y_ssem, y_rsem, device_id={"ep": to_ep}
                 ).start()
 
+    gather(0)
+    experts(0)
+    gather(1)
+    give_back(0)
+    experts(1)
+    give_back(1)
     pltpu.make_async_copy(ysend.at[ep], ret.at[ep], y_rsem).start()
+    landed(ret, y_rsem)
+    picked = jnp.dot(combine[...], ret[...].reshape(slots, LANES), preferred_element_type=f32)
+    routed_sum = picked[:pad_rows] + picked[pad_rows:]
+    mixed_ref[...] = (hid[pl.ds(0, seq_rows), :] + routed_sum[:seq_rows]).astype(bf16)
     landed(hg.at[peers], h_ssem)
     landed(zsend.at[pl.ds(0, n_ep - 1)], z_ssem)
-    for group, (first, last) in enumerate(zip(bounds[:-1], bounds[1:])):
+    for group, (first, last) in enumerate(groups):
         here = pl.ds(2 * first, 2 * (last - first))
         landed(xg.at[peers, here], g_ssem.at[group])
         landed(rsend.at[peers, here], r_ssem.at[group])
     landed(ysend.at[pl.ds(0, n_ep - 1)], y_ssem)
-    landed(ret, y_rsem)
-    picked = jnp.dot(combine[...], ret[...].reshape(slots, LANES), preferred_element_type=f32)
-    routed_sum = picked[:pad_rows] + picked[pad_rows:]
-    mixed_ref[...] = (hid[pl.ds(0, seq_rows), :] + routed_sum[:seq_rows]).astype(bf16)
 
 
 def write_out(*refs):

time: 77 us -> 75.2 us (0.977)
  the two profiles are of different devices: /device:TPU:80 before, /device:TPU:65 now
where the time goes in v5:
time: 75.2 us; the launch traced here: 75 us
  Pallas kernels  74.4 us (99%)
    pallas_call x1, Pallas kernels, shards(): pl.pallas_call(functools.partial(kernel, n_tp, n_ep), out_shape=tuple((pl...  73.7 us

profile of v5, /device:TPU:65, one launch (start us, length us, event | category | flops | bytes accessed | tf_op | source)
XLA Modules:
  0.0 75.0 jit_solution(4076889302058427695)
XLA Ops:
  0.6 73.7 %shard_map.175 = (bf16[10,128]{1,0:T(8,128)(2,1)S(1)}, bf16[10,64]{1,0:T(8,128)(2,1)S(1)}, bf16[10,64]{1,0:T(8,128)(2,1)S(1)}) custom-call(bf16[10,1024]{1,0:T(8,128)(2,1)} %tok_hbm.1, f32[1,1024]{1,0:T(1,128)} %bitcast.20, bf16[1024,128]{1,0:T(8,128)(2,1)} %wq_hbm.1, bf16[64,1024]{1,0:T(8,128)(2,1)} %bitcast.18, bf16[64,1024]{1,0:T(8,128)(2,1)} %bitcast.19, ...), custom_call_target="tpu_custom_call" | custom-call | tf_op jit(solution)/shard_map/pallas_call | solution.py:474
  74.4 0.6 shard_map.176

commit v6 on v5

--- a/solution.py
+++ b/solution.py
@@ -10,6 +10,7 @@
 HEAD_SIZE = 64
 LANES = 128
 CORES = 2
+ALONE = 8
 epsilon = 1e-06
 f32 = jnp.float32
 bf16 = jnp.bfloat16
@@ -156,6 +157,8 @@
     tri[...] = (iota((tri_len, tri_len), 0) > iota((tri_len, tri_len), 1)).astype(f32).astype(bf16)
     rows_pad[...] = jnp.zeros_like(rows_pad)
     hid[...] = jnp.zeros_like(hid)
+    zrecv[pl.ds(1, ALONE - 1)] = jnp.zeros((ALONE - 1, 2, LANES), bf16)
+    zrecv[ALONE + n_ep // 4 - 1] = jnp.zeros((2, LANES), bf16)
     idp[...] = jnp.full(idp.shape, -1.0, f32)
     rwp[...] = jnp.zeros_like(rwp)
 
@@ -272,13 +275,15 @@
     outgoing = jnp.dot(place[...], scaled, preferred_element_type=f32).astype(bf16)
     zsend[...] = outgoing.reshape(zsend.shape)
 
-    bounds = (0, n_ep // 4, n_ep)
-    own_group = jnp.where(ep >= bounds[1], 1, 0)
+    quarter = n_ep // 4
+    groups = ((0, 1, 0, ALONE), (1, quarter, ALONE, quarter), (quarter, n_ep, ALONE + quarter, n_ep - quarter))
+    own_group = jnp.where(ep == 0, 0, jnp.where(ep < quarter, 1, 2))
+    own_entry = jnp.where(ep == 0, 0, jnp.where(ep < quarter, ep + (ALONE - 1), ep + ALONE))
     def send_slots(to_ep):
         @pl.when(to_ep != ep)
         def _():
             pltpu.make_async_remote_copy(
-                zsend.at[to_ep], zrecv.at[ep], z_ssem, z_rsem.at[own_group], device_id={"ep": to_ep}
+                zsend.at[to_ep], zrecv.at[own_entry], z_ssem, z_rsem.at[own_group], device_id={"ep": to_ep}
             ).start()
 
     @pl.when(jnp.logical_not(column))
@@ -304,18 +309,16 @@
         for to_ep in range(max(1, to_chip * CORES), (to_chip + 1) * CORES):
             send_slots(to_ep)
 
-    pltpu.make_async_copy(zsend.at[ep], zrecv.at[ep], z_rsem.at[own_group]).start()
+    pltpu.make_async_copy(zsend.at[ep], zrecv.at[own_entry], z_rsem.at[own_group]).start()
 
     c_wg.wait()
     c_wu.wait()
     c_wd.wait()
-    groups = tuple(zip(bounds[:-1], bounds[1:]))
-
     def gather(group):
-        first, last = groups[group]
-        eps, here = pl.ds(first, last - first), pl.ds(2 * first, 2 * (last - first))
-        landed(zrecv.at[eps], z_rsem.at[group])
-        xg[tp, here] = zrecv[eps].reshape(2 * (last - first), LANES)
+        first, last, entry, width = groups[group]
+        here = pl.ds(2 * entry, 2 * width)
+        landed(zrecv.at[pl.ds(entry, last - first)], z_rsem.at[group])
+        xg[tp, here] = zrecv[pl.ds(entry, width)].reshape(2 * width, LANES)
         for step in far_first(n_tp):
             pltpu.make_async_remote_copy(
                 xg.at[tp, here],
@@ -326,8 +329,7 @@
             ).start()
 
     def experts(group):
-        first, last = groups[group]
-        here = pl.ds(2 * first, 2 * (last - first))
+        here = pl.ds(2 * groups[group][2], 2 * groups[group][3])
         landed(xg.at[peers, here], g_rsem.at[group])
         rows = jnp.concatenate([xg[peer, here] for peer in range(n_tp)], axis=1)
         gate = jnp.dot(rows, wg[...], preferred_element_type=f32)
@@ -349,36 +351,39 @@
         rrecv[tp, here] = rsend[tp, here]
 
     def give_back(group):
-        first, last = groups[group]
-        eps, here = pl.ds(first, last - first), pl.ds(2 * first, 2 * (last - first))
+        first, last, entry, width = groups[group]
+        here = pl.ds(2 * entry, 2 * width)
         landed(rrecv.at[peers, here], r_rsem.at[group])
         total = rrecv[0, here].astype(f32)
         for peer in range(1, n_tp):
             total += rrecv[peer, here].astype(f32)
-        ysend[eps] = total.astype(bf16).reshape(last - first, 2, LANES)
+        ysend[pl.ds(entry, width)] = total.astype(bf16).reshape(width, 2, LANES)
         for to_ep in range(first, last):
 
             @pl.when(to_ep != ep)
             def _():
                 pltpu.make_async_remote_copy(
-                    ysend.at[to_ep], ret.at[ep], y_ssem, y_rsem, device_id={"ep": to_ep}
+                    ysend.at[entry + to_ep - first], ret.at[ep], y_ssem, y_rsem, device_id={"ep": to_ep}
                 ).start()
 
+    gather(1)
     gather(0)
+    experts(1)
     experts(0)
-    gather(1)
+    gather(2)
+    give_back(1)
     give_back(0)
-    experts(1)
-    give_back(1)
-    pltpu.make_async_copy(ysend.at[ep], ret.at[ep], y_rsem).start()
+    experts(2)
+    give_back(2)
+    pltpu.make_async_copy(ysend.at[own_entry], ret.at[ep], y_rsem).start()
     landed(ret, y_rsem)
     picked = jnp.dot(combine[...], ret[...].reshape(slots, LANES), preferred_element_type=f32)
     routed_sum = picked[:pad_rows] + picked[pad_rows:]
     mixed_ref[...] = (hid[pl.ds(0, seq_rows), :] + routed_sum[:seq_rows]).astype(bf16)
     landed(hg.at[peers], h_ssem)
     landed(zsend.at[pl.ds(0, n_ep - 1)], z_ssem)
-    for group, (first, last) in enumerate(groups):
-        here = pl.ds(2 * first, 2 * (last - first))
+    for group, (_, _, entry, width) in enumerate(groups):
+        here = pl.ds(2 * entry, 2 * width)
         landed(xg.at[peers, here], g_ssem.at[group])
         landed(rsend.at[peers, here], r_ssem.at[group])
     landed(ysend.at[pl.ds(0, n_ep - 1)], y_ssem)
@@ -447,21 +452,21 @@
         pltpu.VMEM((LANES, LANES), f32),
         pltpu.VMEM((n_tp, pad_rows, LANES), bf16),
         pltpu.VMEM((n_ep, 2, LANES), bf16),
-        pltpu.VMEM((n_ep, 2, LANES), bf16),
-        pltpu.VMEM((n_tp, slots, LANES), bf16),
-        pltpu.VMEM((n_tp, slots, LANES), bf16),
-        pltpu.VMEM((n_tp, slots, LANES), bf16),
-        pltpu.VMEM((n_ep, 2, LANES), bf16),
+        pltpu.VMEM((n_ep + ALONE, 2, LANES), bf16),
+        pltpu.VMEM((n_tp, slots + 2 * ALONE, LANES), bf16),
+        pltpu.VMEM((n_tp, slots + 2 * ALONE, LANES), bf16),
+        pltpu.VMEM((n_tp, slots + 2 * ALONE, LANES), bf16),
+        pltpu.VMEM((n_ep + ALONE, 2, LANES), bf16),
         pltpu.VMEM((n_ep, 2, LANES), bf16),
         dma((13,)),
         dma,
         dma,
         dma,
-        dma((2,)),
-        dma((2,)),
-        dma((2,)),
-        dma((2,)),
-        dma((2,)),
+        dma((3,)),
+        dma((3,)),
+        dma((3,)),
+        dma((3,)),
+        dma((3,)),
         dma,
         dma,
         pltpu.SemaphoreType.REGULAR((n_ep // CORES,)),

time: 75.2 us -> 73.6 us (0.979)
  the two profiles are of different devices: /device:TPU:65 before, /device:TPU:66 now
where the time goes in v6:
time: 73.6 us; the launch traced here: 73.4 us
  Pallas kernels  72.8 us (99%)
    pallas_call x1, Pallas kernels, shards(): pl.pallas_call(functools.partial(kernel, n_tp, n_ep), out_shape=tuple((pl...  72.2 us

profile of v6, /device:TPU:66, one launch (start us, length us, event | category | flops | bytes accessed | tf_op | source)
XLA Modules:
  0.0 73.4 jit_solution(17434930716896638862)
XLA Ops:
  0.6 72.2 %shard_map.175 = (bf16[10,128]{1,0:T(8,128)(2,1)S(1)}, bf16[10,64]{1,0:T(8,128)(2,1)S(1)}, bf16[10,64]{1,0:T(8,128)(2,1)S(1)}) custom-call(bf16[10,1024]{1,0:T(8,128)(2,1)} %tok_hbm.1, f32[1,1024]{1,0:T(1,128)} %bitcast.20, bf16[1024,128]{1,0:T(8,128)(2,1)} %wq_hbm.1, bf16[64,1024]{1,0:T(8,128)(2,1)} %bitcast.18, bf16[64,1024]{1,0:T(8,128)(2,1)} %bitcast.19, ...), custom_call_target="tpu_custom_call" | custom-call | tf_op jit(solution)/shard_map/pallas_call | solution.py:479
  72.8 0.6 shard_map.176

commit v7 on v6

--- a/solution.py
+++ b/solution.py
@@ -101,6 +101,10 @@
     y_ssem,
     y_rsem,
     ready,
+    psend,
+    terms,
+    p_ssem,
+    p_rsem,
 ):
     tp = lax.axis_index("tp")
     ep = lax.axis_index("ep")
@@ -341,6 +345,26 @@
         up = up * scale
         hidden_act = (gate / (1.0 + jnp.exp(-gate)) * up).astype(bf16)
         partial_value = jnp.dot(hidden_act, wd[...], preferred_element_type=f32).astype(bf16)
+        if group == 0:
+            for c in range(n_tp):
+                psend[c] = partial_value[:2, c * LANES : (c + 1) * LANES]
+            for step in far_first(n_tp):
+                peer = wrap(tp + step, n_tp)
+                pltpu.make_async_remote_copy(
+                    psend.at[peer], terms.at[tp, ep], p_ssem, p_rsem, device_id={"ep": 0, "tp": peer}
+                ).start()
+
+            @pl.when(ep > 0)
+            def _():
+                pltpu.make_async_remote_copy(
+                    psend.at[tp], terms.at[tp, ep], p_ssem, p_rsem, device_id={"ep": 0}
+                ).start()
+
+            @pl.when(ep == 0)
+            def _():
+                pltpu.make_async_copy(psend.at[tp], terms.at[tp, ep], p_rsem).start()
+
+            return
         for c in range(n_tp):
             rsend[c, here] = partial_value[:, c * LANES : (c + 1) * LANES]
         for step in far_first(n_tp):
@@ -372,11 +396,21 @@
     experts(0)
     gather(2)
     give_back(1)
-    give_back(0)
     experts(2)
     give_back(2)
-    pltpu.make_async_copy(ysend.at[own_entry], ret.at[ep], y_rsem).start()
-    landed(ret, y_rsem)
+    @pl.when(ep > 0)
+    def _():
+        pltpu.make_async_copy(ysend.at[own_entry], ret.at[ep], y_rsem).start()
+        landed(ret, y_rsem)
+
+    @pl.when(ep == 0)
+    def _():
+        landed(terms, p_rsem)
+        total = terms[0].astype(f32)
+        for peer in range(1, n_tp):
+            total += terms[peer].astype(f32)
+        ret[...] = total.astype(bf16)
+
     picked = jnp.dot(combine[...], ret[...].reshape(slots, LANES), preferred_element_type=f32)
     routed_sum = picked[:pad_rows] + picked[pad_rows:]
     mixed_ref[...] = (hid[pl.ds(0, seq_rows), :] + routed_sum[:seq_rows]).astype(bf16)
@@ -385,8 +419,18 @@
     for group, (_, _, entry, width) in enumerate(groups):
         here = pl.ds(2 * entry, 2 * width)
         landed(xg.at[peers, here], g_ssem.at[group])
-        landed(rsend.at[peers, here], r_ssem.at[group])
-    landed(ysend.at[pl.ds(0, n_ep - 1)], y_ssem)
+        if group:
+            landed(rsend.at[peers, here], r_ssem.at[group])
+
+    @pl.when(ep > 0)
+    def _():
+        landed(psend, p_ssem)
+        landed(ysend.at[pl.ds(0, n_ep - 2)], y_ssem)
+
+    @pl.when(ep == 0)
+    def _():
+        landed(psend.at[peers], p_ssem)
+        landed(ysend.at[pl.ds(0, n_ep - 1)], y_ssem)
 
 
 def write_out(*refs):
@@ -470,6 +514,10 @@
         dma,
         dma,
         pltpu.SemaphoreType.REGULAR((n_ep // CORES,)),
+        pltpu.VMEM((n_tp, 2, LANES), bf16),
+        pltpu.VMEM((n_tp, n_ep, 2, LANES), bf16),
+        dma,
+        dma,
     ]
     shapes = (
         (seq_rows, w_out.shape[1]),

time: 73.6 us -> 71.5 us (0.971)
  the two profiles are of different devices: /device:TPU:66 before, /device:TPU:80 now
where the time goes in v7:
time: 71.5 us; the launch traced here: 70.2 us
  Pallas kernels  69.6 us (97%)
    pallas_call x1, Pallas kernels, shards(): pl.pallas_call(functools.partial(kernel, n_tp, n_ep), out_shape=tuple((pl...  69 us

profile of v7, /device:TPU:80, one launch (start us, length us, event | category | flops | bytes accessed | tf_op | source)
XLA Modules:
  0.0 70.2 jit_solution(12988927471604503072)
XLA Ops:
  0.6 69.0 %shard_map.175 = (bf16[10,128]{1,0:T(8,128)(2,1)S(1)}, bf16[10,64]{1,0:T(8,128)(2,1)S(1)}, bf16[10,64]{1,0:T(8,128)(2,1)S(1)}) custom-call(bf16[10,1024]{1,0:T(8,128)(2,1)} %tok_hbm.1, f32[1,1024]{1,0:T(1,128)} %bitcast.20, bf16[1024,128]{1,0:T(8,128)(2,1)} %wq_hbm.1, bf16[64,1024]{1,0:T(8,128)(2,1)} %bitcast.18, bf16[64,1024]{1,0:T(8,128)(2,1)} %bitcast.19, ...), custom_call_target="tpu_custom_call" | custom-call | tf_op jit(solution)/shard_map/pallas_call | solution.py:527
  69.6 0.6 shard_map.176

commit v8 on v7

--- a/solution.py
+++ b/solution.py
@@ -294,8 +294,9 @@
     def _():
         send_slots(0)
 
-    for to_chip in range(chips):
-        if to_chip == chips - 1:
+    for turn, far_chip in enumerate(far_first(chips) + [0]):
+        to_chip = jnp.where(ep == 0, far_chip, turn)
+        if turn == chips - 1:
 
             @pl.when(jnp.logical_and(column, ep > 0))
             def _():
@@ -310,8 +311,12 @@
         def _():
             pl.semaphore_wait(ready.at[to_chip], 1)
 
-        for to_ep in range(max(1, to_chip * CORES), (to_chip + 1) * CORES):
-            send_slots(to_ep)
+        for to_core in range(CORES):
+            to_ep = to_chip * CORES + to_core
+
+            @pl.when(to_ep > 0)
+            def _():
+                send_slots(to_ep)
 
     pltpu.make_async_copy(zsend.at[ep], zrecv.at[own_entry], z_rsem.at[own_group]).start()
 

time: 71.5 us -> 71 us (level)
  no operation moved by 1% of the time
where the time goes in v8:
time: 71 us; the launch traced here: 70.2 us
  Pallas kernels  69.6 us (98%)
    pallas_call x1, Pallas kernels, shards(): pl.pallas_call(functools.partial(kernel, n_tp, n_ep), out_shape=tuple((pl...  68.9 us

profile of v8, /device:TPU:80, one launch (start us, length us, event | category | flops | bytes accessed | tf_op | source)
XLA Modules:
  0.0 70.2 jit_solution(15765585161019612625)
XLA Ops:
  0.6 68.9 %shard_map.175 = (bf16[10,128]{1,0:T(8,128)(2,1)S(1)}, bf16[10,64]{1,0:T(8,128)(2,1)S(1)}, bf16[10,64]{1,0:T(8,128)(2,1)S(1)}) custom-call(bf16[10,1024]{1,0:T(8,128)(2,1)} %tok_hbm.1, f32[1,1024]{1,0:T(1,128)} %bitcast.20, bf16[1024,128]{1,0:T(8,128)(2,1)} %wq_hbm.1, bf16[64,1024]{1,0:T(8,128)(2,1)} %bitcast.18, bf16[64,1024]{1,0:T(8,128)(2,1)} %bitcast.19, ...), custom_call_target="tpu_custom_call" | custom-call | tf_op jit(solution)/shard_map/pallas_call | solution.py:532
  69.6 0.6 shard_map.176
